TPU v7x, 32 devices: a whole 2x2x4 slice. The times are simulated.
32 devices in a mesh: ep: 8 (over z, y), tp: 4 (over x, core).
Axes of the slice: x: 2, y: 2, z: 4, core: 2. Of those that a mesh axis runs over, the one named last changes fastest.
Arguments:
- q_heads: bfloat16 [8192, 1024], P('ep', 'tp'), may hold values from -200 to 200
- k_heads: bfloat16 [8192, 256], P('ep', 'tp'), may hold values from -6 to 6
- v_heads: bfloat16 [8192, 256], P('ep', 'tp'), may hold values from -6 to 6
- sink_logits: float32 [16], P('tp'), may hold values from 1 to 5
- out_weight: bfloat16 [1024, 2048], P(None, 'tp'), may hold values from -1.5 to 1.5
- tokens_b: bfloat16 [4096, 2048], P('ep'), may hold values from -6 to 6
- moe_gain: float32 [2048], replicated, may hold values from 0.1 to 1.9
- router_group: bfloat16 [2048, 4], replicated, may hold values from -0.125 to 0.125
- router_expert: bfloat16 [2048, 16], replicated, may hold values from -0.125 to 0.125
- route_expert: int32 [4096, 2], P('ep'), may hold values from 0 to 15, as said below
- expert_gate: bfloat16 [16, 2048, 1024], P('ep', None, 'tp'), may hold values from -0.125 to 0.125
- expert_up: bfloat16 [16, 2048, 1024], P('ep', None, 'tp'), may hold values from -0.125 to 0.125
- expert_down: bfloat16 [16, 1024, 2048], P('ep', 'tp'), may hold values from -0.75 to 0.75
Outputs:
- mixer_out: bfloat16 [8192, 2048], P('ep', 'tp')
- moe_out: bfloat16 [4096, 2048], P(('ep', 'tp'))
Inputs may be any that keep to these rules, and one draw needn't show every extreme that they name: `route_expert`: each token names two different experts, in rising order, of one group of 4 consecutive experts. In each aligned block of 128 rows (the rows of one device) no expert is named by more than 32 tokens, in each group one expert is named by exactly 32 tokens of every block, and each group is named by a quarter of every block's tokens.
All inputs are finite; a program needn't handle non-finite values.
Results may differ from a plain program's by a relative error of at most 0.011.
Values may be sent and summed in bfloat16 or wider, within the bound.
A program may use at most 128 MiB of HBM per device.

v0:
```python
import functools

import jax
import jax.numpy as jnp
from jax import lax
from jax.experimental import pallas as pl
from jax.experimental.pallas import tpu as pltpu
from jax.sharding import PartitionSpec as P

HEADS = 16
KV = 4
HD = 64
WINDOW = 128


def shifted(value, axis, steps):
    count = lax.axis_size(axis)
    leading, last = (max(0, -steps), min(count, count - steps))
    return lax.ppermute(value, axis, [(source, source + steps) for source in range(leading, last)])


def normalize(rows_in, gain):
    values = rows_in.astype(jnp.float32)
    scaled = values * lax.rsqrt(jnp.mean(values * values, axis=-1, keepdims=True) + 1e-06) * gain
    return scaled.astype(jnp.bfloat16)


def gate_weights(normed, routes, router_group, router_expert):
    group_logits = jnp.dot(normed, router_group, preferred_element_type=jnp.float32)
    expert_logits = jnp.dot(normed, router_expert, preferred_element_type=jnp.float32)
    group_count = router_group.shape[1]
    expert_count = router_expert.shape[1]
    chosen_group = routes[:, 0] // (expert_count // group_count)
    group_match = chosen_group[:, None] == jnp.arange(group_count, dtype=jnp.int32)[None, :]
    group_share = jnp.sum(
        jnp.where(group_match, jax.nn.softmax(group_logits, axis=-1), 0.0), axis=-1
    )
    expert_match = routes[:, :, None] == jnp.arange(expert_count, dtype=jnp.int32)[None, None, :]
    picked = jnp.sum(jnp.where(expert_match, expert_logits[:, None, :], 0.0), axis=-1)
    return group_share[:, None] * jax.nn.softmax(picked, axis=-1)


def slot_positions(routes, sub_count, expert_count):
    flat_routes = routes.reshape(sub_count, -1)
    onehot = (
        flat_routes[:, :, None] == jnp.arange(expert_count, dtype=jnp.int32)[None, None, :]
    ).astype(jnp.int32)
    places = jnp.sum(onehot * jnp.cumsum(onehot, axis=1), axis=2) - 1
    return (flat_routes, places)


def fill_slots(normed, flat_routes, places, sub_count, expert_count, capacity, exp_local):
    sub_index = jnp.arange(sub_count, dtype=jnp.int32)[:, None]
    target = ((flat_routes * sub_count + sub_index) * capacity + places).reshape(-1)
    source = jnp.repeat(normed, 2, axis=0)
    buffer = jnp.zeros((expert_count * sub_count * capacity, normed.shape[1]), jnp.bfloat16)
    buffer = buffer.at[target].set(source)
    return buffer.reshape(
        expert_count // exp_local, exp_local, sub_count, capacity, normed.shape[1]
    )


LANES = 128
MESH = pl.DeviceIdType.MESH


def fused_kernel(
    groups,
    sink_ref,
    q_ref,
    k_ref,
    v_ref,
    gain_ref,
    group_ref,
    expert_ref,
    route_ref,
    tokens_hbm,
    gate_hbm,
    up_hbm,
    down_hbm,
    proj_hbm,
    mixer_ref,
    out_ref,
    k_ext,
    v_ext,
    tokens,
    xs_ref,
    heads,
    rows,
    part,
    wg,
    wu,
    wd,
    proj,
    act,
    from_core,
    relay_x,
    relay_y,
    from_x,
    from_y,
    total,
    back,
    load_sem,
    send_sem,
    recv_sem,
):
    ep, tp = lax.axis_index("ep"), lax.axis_index("tp")
    group, member = ep // 2, ep % 2
    x, core = tp // 2, tp % 2
    tp_x, tp_c = (1 - x) * 2 + core, x * 2 + (1 - core)
    ep_y = group * 2 + (1 - member)
    ep_count = groups * 2
    x_dev, y_dev, c_dev = (ep, tp_x), (ep_y, tp), (ep, tp_c)
    next_dev = ((ep + 1) % ep_count, tp)
    prev_dev = ((ep + ep_count - 1) % ep_count, tp)
    depth = out_ref.shape[1]
    chunk = xs_ref.shape[0] // groups
    half = chunk // 2
    row_count = q_ref.shape[0]
    lo, hi = pl.ds(0, half), pl.ds(half, half)
    mine, other = core * 4, (1 - core) * 4
    own = mine + member * 2 + x
    slot_x = mine + member * 2 + (1 - x)
    slot_y = mine + (1 - member) * 2 + x
    slot_d = mine + (1 - member) * 2 + (1 - x)
    mine_slots, other_slots = pl.ds(mine, 4), pl.ds(other, 4)

    pairs = ((gate_hbm, wg), (up_hbm, wu), (down_hbm, wd), (proj_hbm, proj))
    loads = [
        pltpu.make_async_copy(source, held, load_sem.at[i])
        for i, (source, held) in enumerate(pairs)
    ]
    block = xs_ref.shape[0]
    first = pl.multiple_of(tp * block, block)
    fetch = pltpu.make_async_copy(tokens_hbm.at[pl.ds(first, block)], tokens, load_sem.at[5])
    fetch.start()
    for load in loads:
        load.start()

    barrier = pltpu.get_barrier_semaphore()
    ahead = [((group + step) % groups) * 2 + member for step in range(1, groups)]
    peers = [(plane, tp) for plane in ahead] + [x_dev, y_dev, c_dev, next_dev, prev_dev]
    for peer in peers:
        pl.semaphore_signal(barrier, inc=1, device_id=peer, device_id_type=MESH)
    fetch.wait()
    values = tokens[...].astype(jnp.float32)
    scale = lax.rsqrt(jnp.mean(values * values, axis=1, keepdims=True) + 1e-06)
    normed = (values * scale * gain_ref[...]).astype(jnp.bfloat16)
    across = (((1,), (1,)), ((), ()))
    group_logits = lax.dot_general(
        group_ref[...], normed, across, preferred_element_type=jnp.float32
    )
    expert_logits = lax.dot_general(
        expert_ref[...], normed, across, preferred_element_type=jnp.float32
    )
    routes = route_ref[:, pl.ds(first, block)]
    route_a, route_b = routes[0:1], routes[1:2]
    group_experts = expert_ref.shape[0] // groups
    group_at = lax.broadcasted_iota(jnp.int32, (groups, block), 0)
    inside = route_a - group_at * group_experts
    named = (inside >= 0) & (inside < group_experts)
    group_exp = jnp.exp(group_logits - jnp.max(group_logits, axis=0, keepdims=True))
    group_share = jnp.sum(jnp.where(named, group_exp, 0.0), axis=0, keepdims=True) / jnp.sum(
        group_exp, axis=0, keepdims=True
    )
    expert_at = lax.broadcasted_iota(jnp.int32, expert_logits.shape, 0)
    logit_a = jnp.sum(jnp.where(expert_at == route_a, expert_logits, 0.0), axis=0, keepdims=True)
    logit_b = jnp.sum(jnp.where(expert_at == route_b, expert_logits, 0.0), axis=0, keepdims=True)
    top = jnp.maximum(logit_a, logit_b)
    exp_a, exp_b = jnp.exp(logit_a - top), jnp.exp(logit_b - top)
    gate_a = group_share * (exp_a / (exp_a + exp_b))
    gate_b = group_share * (exp_b / (exp_a + exp_b))
    base = jnp.sum(jnp.where(named, group_at * group_experts, 0), axis=0, keepdims=True)
    lane_at = lax.broadcasted_iota(jnp.int32, (LANES // 2, block), 0)
    share_t = jnp.where(lane_at == route_a - base, gate_a, 0.0) + jnp.where(
        lane_at == route_b - base, gate_b, 0.0
    )
    coarse = share_t.astype(jnp.bfloat16)
    fine = (share_t - coarse.astype(jnp.float32)).astype(jnp.bfloat16)
    row_at = lax.broadcasted_iota(jnp.int32, (block, block), 0)
    column_at = lax.broadcasted_iota(jnp.int32, (block, block), 1)
    earlier = jnp.where(row_at < column_at, 1.0, 0.0).astype(jnp.bfloat16)
    counts = jnp.dot(
        jnp.where(named, 1.0, 0.0).astype(jnp.bfloat16), earlier, preferred_element_type=jnp.float32
    )
    first_row = (group_at * chunk).astype(jnp.float32)
    place = jnp.sum(jnp.where(named, counts + first_row, 0.0), axis=0, keepdims=True)
    take = jnp.where(row_at.astype(jnp.float32) == place, 1.0, 0.0).astype(jnp.bfloat16)
    xs_ref[:, :depth] = jnp.dot(take, normed, preferred_element_type=jnp.float32).astype(
        jnp.bfloat16
    )
    xs_ref[:, depth:] = lax.dot_general(
        take, jnp.concatenate([coarse, fine], axis=0), across, preferred_element_type=jnp.float32
    ).astype(jnp.bfloat16)
    pl.semaphore_wait(barrier, len(peers))

    started = []

    def send(source, target, device):
        index = len(started)
        copy = pltpu.make_async_remote_copy(
            src_ref=source,
            dst_ref=target,
            send_sem=send_sem.at[index],
            recv_sem=recv_sem.at[index],
            device_id=device,
            device_id_type=MESH,
        )
        copy.start()
        started.append(copy)
        return copy

    my_chunk = pl.ds(pl.multiple_of(group * chunk, chunk), chunk)
    keep = pltpu.make_async_copy(xs_ref.at[my_chunk], rows.at[0, own], load_sem.at[4])
    keep.start()
    tail = pl.ds(row_count - WINDOW, WINDOW)
    halo = [
        send(source.at[:, tail], target.at[:, pl.ds(0, WINDOW)], next_dev)
        for source, target in ((k_ref, k_ext), (v_ref, v_ext))
    ]
    z_out = [keep]
    for step in range(1, groups):
        plane = (group + step) % groups
        there = pl.ds(pl.multiple_of(plane * chunk, chunk), chunk)
        z_out.append(send(xs_ref.at[there], rows.at[step, own], (plane * 2 + member, tp)))
    k_ext[:, pl.ds(WINDOW, row_count)] = k_ref[...]
    v_ext[:, pl.ds(WINDOW, row_count)] = v_ref[...]

    held = [dict() for _ in range(groups)]

    def stage_a(s):
        if s:
            z_out[s].wait_recv()
        else:
            keep.wait()
        held[s]["x"] = send(rows.at[s, own], rows.at[s, own], x_dev)
        held[s]["y"] = send(rows.at[s, own], rows.at[s, own], y_dev)

    def stage_b(s):
        held[s]["x"].wait_recv()
        held[s]["to_y"] = send(rows.at[s, slot_x], rows.at[s, slot_x], y_dev)

    def stage_c(s):
        held[s]["y"].wait_recv()
        held[s]["to_y"].wait_recv()
        held[s]["core"] = send(rows.at[s, mine_slots], rows.at[s, mine_slots], c_dev)

    def stage_d(s):
        held[s]["core"].wait_recv()
        batch = 8 * chunk
        tokens = rows[s, :, :, :depth].reshape(batch, depth)
        shares = rows[s, :, :, depth:].reshape(batch, LANES).astype(jnp.float32)
        lane = lax.broadcasted_iota(jnp.int32, shares.shape, 1) % (LANES // 2)

        def one(e, carry):
            share = jnp.sum(
                jnp.where(lane == member * wg.shape[0] + e, shares, 0.0), axis=1, keepdims=True
            )
            pre = jnp.dot(tokens, wg[e], preferred_element_type=jnp.float32)
            up = jnp.dot(tokens, wu[e], preferred_element_type=jnp.float32)
            act[e] = (jax.nn.silu(pre) * up * share).astype(jnp.bfloat16)
            return carry

        lax.fori_loop(0, wg.shape[0], one, 0)
        acts = jnp.concatenate([act[e] for e in range(wg.shape[0])], axis=1)
        tile = 512

        def column(n, carry):
            columns = pl.ds(pl.multiple_of(n * tile, tile), tile)
            value = jnp.dot(acts, wd[:, columns], preferred_element_type=jnp.float32)
            part[s, :, :, columns] = value.astype(jnp.bfloat16).reshape(8, chunk, tile)
            return carry

        lax.fori_loop(0, depth // tile, column, 0)
        held[s]["sum"] = send(part.at[s, other_slots], from_core.at[s], c_dev)

    def add(index, term):
        part[index] = (part[index].astype(jnp.float32) + term.astype(jnp.float32)).astype(
            jnp.bfloat16
        )

    def stage_e(s):
        held[s]["sum"].wait_recv()
        add((s, mine_slots), from_core[s])
        held[s]["d_y"] = send(part.at[s, slot_d, lo], relay_y.at[s], y_dev)
        held[s]["d_x"] = send(part.at[s, slot_d, hi], relay_x.at[s], x_dev)
        held[s]["x_hi"] = send(part.at[s, slot_x, hi], from_x.at[s, hi], x_dev)
        held[s]["y_lo"] = send(part.at[s, slot_y, lo], from_y.at[s, lo], y_dev)

    def stage_f(s):
        held[s]["d_y"].wait_recv()
        add((s, slot_x, lo), relay_y[s])
        held[s]["x_lo"] = send(part.at[s, slot_x, lo], from_x.at[s, lo], x_dev)
        held[s]["d_x"].wait_recv()
        add((s, slot_y, hi), relay_x[s])
        held[s]["y_hi"] = send(part.at[s, slot_y, hi], from_y.at[s, hi], y_dev)

    def stage_h(s):
        for name in ("x_hi", "y_lo", "x_lo", "y_hi"):
            held[s][name].wait_recv()
        summed = (
            part[s, own].astype(jnp.float32)
            + from_x[s].astype(jnp.float32)
            + from_y[s].astype(jnp.float32)
        ).astype(jnp.bfloat16)
        if s:
            total[s] = summed
            plane = (group + groups - s) % groups
            held[s]["home"] = send(total.at[s], back.at[my_chunk], (plane * 2 + member, tp))
        else:
            back[my_chunk] = summed

    head_count = q_ref.shape[1] // HD
    query_at = lax.broadcasted_iota(jnp.int32, (WINDOW, 2 * WINDOW), 0)
    key_at = lax.broadcasted_iota(jnp.int32, (WINDOW, 2 * WINDOW), 1)
    distance = query_at + WINDOW - key_at
    near = (distance >= 0) & (distance < WINDOW)

    def attend(b, carry):
        start = pl.multiple_of(b * WINDOW, WINDOW)
        keys = k_ext[:, pl.ds(start, 2 * WINDOW)]
        band = v_ext[:, pl.ds(start, 2 * WINDOW)]
        queries = q_ref[pl.ds(start, WINDOW)]
        allowed = near & (key_at + (ep * row_count + b * WINDOW - WINDOW) >= 0)
        outs = []
        for h in range(head_count):
            query = queries[:, h * HD : (h + 1) * HD]
            scores = jnp.dot(query, keys, preferred_element_type=jnp.float32) * HD ** (-0.5)
            masked = jnp.where(allowed, scores, -1e30)
            sink = jnp.full((WINDOW, 1), sink_ref[h], jnp.float32)
            row_max = jnp.maximum(jnp.max(masked, axis=1, keepdims=True), sink)
            weights = jnp.exp(masked - row_max)
            denominator = jnp.sum(weights, axis=1, keepdims=True) + jnp.exp(sink - row_max)
            probs = (weights * (1.0 / denominator)).astype(jnp.bfloat16)
            outs.append(lax.dot_general(probs, band, across, preferred_element_type=jnp.float32))
        heads[tp, pl.ds(start, WINDOW)] = jnp.concatenate(outs, axis=1).astype(jnp.bfloat16)
        return carry

    blocks = row_count // WINDOW
    piece = row_count // 4
    att_x = []

    def send_heads(i):
        span = pl.ds(i * piece, piece)
        att_x.append(send(heads.at[tp, span], heads.at[tp, span], x_dev))

    stage_a(0)
    lax.fori_loop(1, blocks // 2, attend, 0)
    stage_b(0)
    stage_a(1)
    lax.fori_loop(blocks // 2, blocks, attend, 0)
    stage_c(0)
    stage_b(1)
    stage_a(2)
    for copy in halo:
        copy.wait_recv()
    lax.fori_loop(0, 1, attend, 0)
    send_heads(0)
    att_c = send(heads.at[tp], heads.at[tp], c_dev)
    for load in loads:
        load.wait()
    stage_d(0)
    stage_c(1)
    stage_b(2)
    stage_a(3)
    stage_e(0)
    stage_d(1)
    send_heads(1)
    stage_f(0)
    stage_c(2)
    stage_b(3)
    stage_e(1)
    stage_d(2)
    stage_h(0)
    send_heads(2)
    stage_f(1)
    stage_c(3)
    stage_e(2)
    stage_d(3)
    stage_h(1)
    stage_f(2)
    stage_e(3)
    send_heads(3)
    stage_h(2)
    stage_f(3)
    for copy in att_x:
        copy.wait_recv()
    att_cx = send(heads.at[tp_x], heads.at[tp_x], c_dev)
    att_c.wait_recv()
    att_cx.wait_recv()
    stage_h(3)

    def project(i, carry):
        span = pl.ds(pl.multiple_of(i * piece, piece), piece)
        joined = jnp.concatenate([heads[t, span] for t in range(4)], axis=1)
        mixer_ref[span] = jnp.dot(joined, proj[...], preferred_element_type=jnp.float32).astype(
            jnp.bfloat16
        )
        return carry

    lax.fori_loop(0, 4, project, 0)
    for s in range(1, groups):
        held[s]["home"].wait_recv()
    out_ref[...] = lax.dot_general(
        take, back[...], (((0,), (0,)), ((), ())), preferred_element_type=jnp.float32
    ).astype(jnp.bfloat16)
    for copy in started:
        copy.wait_send()


def fused(
    sinks,
    q_heads,
    k_heads,
    v_heads,
    gain,
    router_group,
    router_expert,
    routes,
    tokens_b,
    expert_gate,
    expert_up,
    expert_down,
    proj,
):
    groups = router_group.shape[1]
    block = tokens_b.shape[0] // 4
    experts, depth, hidden = expert_gate.shape
    width = depth + LANES
    row_count, head_width = q_heads.shape
    down = expert_down.reshape(experts * hidden, depth)
    chunk = block // groups
    copies = 14 * groups + 8
    bf16 = jnp.bfloat16
    anywhere = pl.BlockSpec(memory_space=pl.ANY)
    vmem = pl.BlockSpec(memory_space=pltpu.VMEM)
    return pl.pallas_call(
        functools.partial(fused_kernel, groups),
        out_shape=(
            jax.ShapeDtypeStruct((row_count, proj.shape[1]), bf16),
            jax.ShapeDtypeStruct((block, depth), bf16),
        ),
        in_specs=[pl.BlockSpec(memory_space=pltpu.SMEM)] + [vmem] * 7 + [anywhere] * 5,
        out_specs=(vmem, vmem),
        scratch_shapes=[
            pltpu.VMEM((HD, row_count + WINDOW), bf16),
            pltpu.VMEM((HD, row_count + WINDOW), bf16),
            pltpu.VMEM((block, depth), bf16),
            pltpu.VMEM((block, width), bf16),
            pltpu.VMEM((4, row_count, head_width), bf16),
            pltpu.VMEM((groups, 8, chunk, width), bf16),
            pltpu.VMEM((groups, 8, chunk, depth), bf16),
            pltpu.VMEM(expert_gate.shape, bf16),
            pltpu.VMEM(expert_up.shape, bf16),
            pltpu.VMEM(down.shape, bf16),
            pltpu.VMEM(proj.shape, bf16),
            pltpu.VMEM((experts, 8 * chunk, hidden), bf16),
            pltpu.VMEM((groups, 4, chunk, depth), bf16),
            pltpu.VMEM((groups, chunk // 2, depth), bf16),
            pltpu.VMEM((groups, chunk // 2, depth), bf16),
            pltpu.VMEM((groups, chunk, depth), bf16),
            pltpu.VMEM((groups, chunk, depth), bf16),
            pltpu.VMEM((groups, chunk, depth), bf16),
            pltpu.VMEM((block, depth), bf16),
            pltpu.SemaphoreType.DMA((6,)),
            pltpu.SemaphoreType.DMA((copies,)),
            pltpu.SemaphoreType.DMA((copies,)),
        ],
        cost_estimate=pl.CostEstimate(
            flops=20_000_000_000, bytes_accessed=20_000_000, transcendentals=0
        ),
        compiler_params=pltpu.CompilerParams(
            collective_id=0, has_side_effects=True, vmem_limit_bytes=56 * 2**20
        ),
    )(
        sinks,
        q_heads,
        k_heads.T,
        v_heads.T,
        gain[None, :],
        router_group.T,
        router_expert.T,
        routes.T,
        tokens_b,
        expert_gate,
        expert_up,
        down,
        proj,
    )


def per_device(
    q_heads,
    k_heads,
    v_heads,
    sink_logits,
    out_weight,
    tokens_b,
    moe_gain,
    router_group,
    router_expert,
    route_expert,
    expert_gate,
    expert_up,
    expert_down,
):
    groups = router_group.shape[1]
    if (lax.axis_size("ep"), lax.axis_size("tp"), k_heads.shape[1]) == (2 * groups, 4, HD):
        return fused(
            sink_logits,
            q_heads,
            k_heads,
            v_heads,
            moe_gain,
            router_group,
            router_expert,
            route_expert,
            tokens_b,
            expert_gate,
            expert_up,
            expert_down,
            out_weight,
        )
    span_len = WINDOW
    row_count = q_heads.shape[0]
    kv_local = k_heads.shape[1] // HD
    group_size = HEADS // KV
    blocks = row_count // span_len
    stacked = jnp.stack([k_heads[row_count - span_len :], v_heads[row_count - span_len :]])
    earlier = shifted(stacked, "ep", 1)

    def make_band(own_rows, prev_rows):
        extended = jnp.concatenate([prev_rows, own_rows], axis=0).reshape(
            blocks + 1, span_len, kv_local, HD
        )
        return jnp.concatenate([extended[:-1], extended[1:]], axis=1)

    key_band = make_band(k_heads, earlier[0])
    value_band = make_band(v_heads, earlier[1])
    query_blocks = q_heads.reshape(blocks, span_len, kv_local, group_size, HD)
    scores = jnp.einsum(
        "nqhgd,nkhd->nhgqk", query_blocks, key_band, preferred_element_type=jnp.float32
    ) * HD ** (-0.5)
    first_row = lax.axis_index("ep") * row_count
    query_index = jnp.arange(span_len, dtype=jnp.int32)[:, None]
    key_index = jnp.arange(2 * span_len, dtype=jnp.int32)[None, :]
    distance = query_index + span_len - key_index
    key_place = (
        first_row
        + jnp.arange(blocks, dtype=jnp.int32)[:, None, None] * span_len
        + key_index[None]
        - span_len
    )
    allowed = (distance >= 0)[None] & (distance < span_len)[None] & (key_place >= 0)
    masked = jnp.where(allowed[:, None, None], scores, -1e30)
    sink_full = sink_logits.reshape(kv_local, group_size)[None, :, :, None]
    row_max = jnp.maximum(jnp.max(masked, axis=-1), sink_full)
    weights_exp = jnp.exp(masked - row_max[..., None])
    denominator = jnp.sum(weights_exp, axis=-1) + jnp.exp(sink_full - row_max)
    probs = (weights_exp / denominator[..., None]).astype(jnp.bfloat16)
    attended = jnp.einsum(
        "nhgqk,nkhd->nqhgd", probs, value_band, preferred_element_type=jnp.float32
    )
    attended = attended.astype(jnp.bfloat16).reshape(row_count, kv_local * group_size * HD)
    mixed = jnp.dot(
        lax.all_gather(attended, "tp", axis=1, tiled=True),
        out_weight,
        preferred_element_type=jnp.float32,
    )
    mixer_out = mixed.astype(jnp.bfloat16)
    tp_count = lax.axis_size("tp")
    tp_index = lax.axis_index("tp")
    exp_local = expert_gate.shape[0]
    expert_count = exp_local * lax.axis_size("ep")
    rows_dev = tokens_b.shape[0] // tp_count
    capacity = min(4 * rows_dev // expert_count, rows_dev // 4)
    own_routes = lax.dynamic_slice_in_dim(route_expert, tp_index * rows_dev, rows_dev, 0)
    own_normed = normalize(
        lax.dynamic_slice_in_dim(tokens_b, tp_index * rows_dev, rows_dev, 0), moe_gain
    )
    flat_routes, places = slot_positions(own_routes, 1, expert_count)
    buffer = fill_slots(own_normed, flat_routes, places, 1, expert_count, capacity, exp_local)
    delivered = lax.all_to_all(buffer, "ep", split_axis=0, concat_axis=0, tiled=True)
    arrived = lax.all_gather(delivered, "tp", axis=2, tiled=True)
    own_flat = flat_routes[0]
    own_places = places[0]
    gates = gate_weights(own_normed, own_routes, router_group, router_expert)
    gate_pre = jnp.einsum(
        "setcd,edf->setcf", arrived, expert_gate, preferred_element_type=jnp.float32
    )
    up_pre = jnp.einsum("setcd,edf->setcf", arrived, expert_up, preferred_element_type=jnp.float32)
    activated = (jax.nn.silu(gate_pre) * up_pre).astype(jnp.bfloat16)
    partial_value = jnp.einsum(
        "setcf,efd->setcd", activated, expert_down, preferred_element_type=jnp.float32
    )
    summed = lax.psum_scatter(
        partial_value.astype(jnp.bfloat16), "tp", scatter_dimension=2, tiled=True
    )
    returned = lax.all_to_all(summed, "ep", split_axis=0, concat_axis=0, tiled=True)
    returned = returned.reshape(expert_count * capacity, returned.shape[-1])
    picked_rows = returned[own_flat * capacity + own_places].reshape(
        rows_dev, 2, returned.shape[-1]
    )
    moe_out = jnp.sum(gates[:, :, None] * picked_rows.astype(jnp.float32), axis=1).astype(
        jnp.bfloat16
    )
    return (mixer_out, moe_out)


def solution(mesh):
    in_specs = (
        P("ep", "tp"),
        P("ep", "tp"),
        P("ep", "tp"),
        P("tp"),
        P(None, "tp"),
        P("ep", None),
        P(),
        P(),
        P(),
        P("ep", None),
        P("ep", None, "tp"),
        P("ep", None, "tp"),
        P("ep", "tp", None),
    )
    out_specs = (P("ep", "tp"), P(("ep", "tp"), None))
    return jax.shard_map(
        per_device, mesh=mesh, in_specs=in_specs, out_specs=out_specs, check_vma=False
    )
```

profile of v0, /device:TPU:0, one launch (start us, length us, event | category | flops | bytes accessed | tf_op | source)
XLA Modules:
  0.0 68.9 jit_solution(522516714036971327)
XLA Ops:
  0.6 65.1 %shard_map.140 = (bf16[1024,512]{1,0:T(8,128)(2,1)}, bf16[128,2048]{1,0:T(8,128)(2,1)}) custom-call(f32[4]{0:T(128)} %sink_ref.1, bf16[1024,256]{1,0:T(8,128)(2,1)} %q_ref.1, bf16[64,1024]{1,0:T(8,128)(2,1)} %bitcast.8, bf16[64,1024]{1,0:T(8,128)(2,1)} %bitcast.9, f32[1,2048]{1,0:T(1,128)} %bitcast.12, bf16[4,2048]{1,0:T(4,128)(2,1)} %bitcast.11, ...), custom_call_target="tpu_custom_call" | custom-call | flops 20000000000 | bytes 20000000 | tf_op jit(solution)/shard_map/pallas_call | solution.py:437
  65.8 0.0 copy-start
  65.8 2.3 %copy.17 = bf16[1024,512]{1,0:T(8,128)(2,1)} copy(bf16[1024,512]{1,0:T(8,128)(2,1)} %get-tuple-element.4) | data formatting | bytes 2097152
  68.1 0.0 copy-done
  68.1 0.8 %copy.18 = bf16[128,2048]{1,0:T(8,128)(2,1)} copy(bf16[128,2048]{1,0:T(8,128)(2,1)S(1)} %copy-done) | data formatting | bytes 1048576
Async XLA Ops:
  65.8 2.3 %copy-start = (bf16[128,2048]{1,0:T(8,128)(2,1)S(1)}, bf16[128,2048]{1,0:T(8,128)(2,1)}, u32[]{:S(2)}) copy-start(bf16[128,2048]{1,0:T(8,128)(2,1)} %get-tuple-element.5) | copy-start | bytes 1572868
where the time goes:
time: 69.1 us; the launch traced here: 68.9 us
  Pallas kernels  65.1 us (94%)
  local copies, waits for them, and re-layouts  3.12 us (5%)
    pallas_call x1, Pallas kernels, fused(): pl.pallas_call(functools.partial(fused_kernel, groups), out_shape=(jax.Sh...  65.1 us
    unnamed x4, local copies, waits for them, and re-layouts  3.12 us

commit v1 on v0

--- a/solution.py
+++ b/solution.py
@@ -62,25 +62,46 @@
 
 LANES = 128
 MESH = pl.DeviceIdType.MESH
+NS = jax.named_scope
+FIRST = "0"
+SENDERS = 24
+RECEIVERS = 52
+
+
+def UNITS(chunk):
+    half = chunk // 2
+    return {
+        "0": (0, 0, chunk),
+        "1": (1, 0, chunk),
+        "2": (2, 0, chunk),
+        "a": (3, 0, half),
+        "b": (3, half, half),
+    }
 
 
 def fused_kernel(
     groups,
-    sink_ref,
-    q_ref,
-    k_ref,
-    v_ref,
-    gain_ref,
-    group_ref,
-    expert_ref,
-    route_ref,
+    sink_hbm,
+    q_hbm,
+    k_hbm,
+    v_hbm,
+    gain_hbm,
+    group_hbm,
+    expert_hbm,
+    route_hbm,
     tokens_hbm,
     gate_hbm,
     up_hbm,
     down_hbm,
     proj_hbm,
-    mixer_ref,
-    out_ref,
+    mixer_hbm,
+    out_hbm,
+    sink_ref,
+    q_ref,
+    gain_ref,
+    group_ref,
+    expert_ref,
+    route_ref,
     k_ext,
     v_ext,
     tokens,
@@ -96,11 +117,13 @@
     from_core,
     relay_x,
     relay_y,
-    from_x,
-    from_y,
+    from_xy,
     total,
     back,
+    mixed,
+    moved,
     load_sem,
+    out_sem,
     send_sem,
     recv_sem,
 ):
@@ -113,11 +136,10 @@
     x_dev, y_dev, c_dev = (ep, tp_x), (ep_y, tp), (ep, tp_c)
     next_dev = ((ep + 1) % ep_count, tp)
     prev_dev = ((ep + ep_count - 1) % ep_count, tp)
-    depth = out_ref.shape[1]
-    chunk = xs_ref.shape[0] // groups
-    half = chunk // 2
+    depth = back.shape[1]
+    block = xs_ref.shape[0]
+    chunk = block // groups
     row_count = q_ref.shape[0]
-    lo, hi = pl.ds(0, half), pl.ds(half, half)
     mine, other = core * 4, (1 - core) * 4
     own = mine + member * 2 + x
     slot_x = mine + member * 2 + (1 - x)
@@ -125,24 +147,44 @@
     slot_d = mine + (1 - member) * 2 + (1 - x)
     mine_slots, other_slots = pl.ds(mine, 4), pl.ds(other, 4)
 
-    pairs = ((gate_hbm, wg), (up_hbm, wu), (down_hbm, wd), (proj_hbm, proj))
+    def plane(step):
+        return (group + step) % groups
+
+    barrier = pltpu.get_barrier_semaphore()
+    ahead = [plane(step) * 2 + member for step in range(1, groups)]
+    peers = [(there, tp) for there in ahead] + [x_dev, y_dev, c_dev, next_dev, prev_dev]
+    for peer in peers:
+        pl.semaphore_signal(barrier, inc=1, device_id=peer, device_id_type=MESH)
+
+    first = pl.multiple_of(tp * block, block)
+    inner = pl.ds(WINDOW, row_count)
+    pairs = (
+        (tokens_hbm.at[pl.ds(first, block)], tokens),
+        (gain_hbm, gain_ref),
+        (group_hbm, group_ref),
+        (expert_hbm, expert_ref),
+        (route_hbm.at[:, pl.ds(first, block)], route_ref),
+        (k_hbm, k_ext.at[:, inner]),
+        (v_hbm, v_ext.at[:, inner]),
+        (q_hbm, q_ref),
+        (sink_hbm, sink_ref),
+        (gate_hbm, wg),
+        (up_hbm, wu),
+        (down_hbm, wd),
+        (proj_hbm, proj),
+    )
     loads = [
         pltpu.make_async_copy(source, held, load_sem.at[i])
         for i, (source, held) in enumerate(pairs)
     ]
-    block = xs_ref.shape[0]
-    first = pl.multiple_of(tp * block, block)
-    fetch = pltpu.make_async_copy(tokens_hbm.at[pl.ds(first, block)], tokens, load_sem.at[5])
-    fetch.start()
-    for load in loads:
+    early, middle, late = loads[:5], loads[5:9], loads[9:]
+    for load in early + middle:
         load.start()
-
-    barrier = pltpu.get_barrier_semaphore()
-    ahead = [((group + step) % groups) * 2 + member for step in range(1, groups)]
-    peers = [(plane, tp) for plane in ahead] + [x_dev, y_dev, c_dev, next_dev, prev_dev]
-    for peer in peers:
-        pl.semaphore_signal(barrier, inc=1, device_id=peer, device_id_type=MESH)
-    fetch.wait()
+    with NS("wearly"):
+        for load in early:
+            load.wait()
+    for load in late:
+        load.start()
     values = tokens[...].astype(jnp.float32)
     scale = lax.rsqrt(jnp.mean(values * values, axis=1, keepdims=True) + 1e-06)
     normed = (values * scale * gain_ref[...]).astype(jnp.bfloat16)
@@ -153,7 +195,7 @@
     expert_logits = lax.dot_general(
         expert_ref[...], normed, across, preferred_element_type=jnp.float32
     )
-    routes = route_ref[:, pl.ds(first, block)]
+    routes = route_ref[...]
     route_a, route_b = routes[0:1], routes[1:2]
     group_experts = expert_ref.shape[0] // groups
     group_at = lax.broadcasted_iota(jnp.int32, (groups, block), 0)
@@ -192,123 +234,186 @@
     xs_ref[:, depth:] = lax.dot_general(
         take, jnp.concatenate([coarse, fine], axis=0), across, preferred_element_type=jnp.float32
     ).astype(jnp.bfloat16)
-    pl.semaphore_wait(barrier, len(peers))
-
-    started = []
-
-    def send(source, target, device):
-        index = len(started)
-        copy = pltpu.make_async_remote_copy(
+    with NS("barrier"):
+        pl.semaphore_wait(barrier, len(peers))
+
+    in_flight, used, names = {}, [0], {}
+
+    def descriptor(source, target, device, sender, name):
+        receiver = names.setdefault(name, len(names))
+        return pltpu.make_async_remote_copy(
             src_ref=source,
             dst_ref=target,
-            send_sem=send_sem.at[index],
-            recv_sem=recv_sem.at[index],
+            send_sem=send_sem.at[sender],
+            recv_sem=recv_sem.at[receiver],
             device_id=device,
             device_id_type=MESH,
         )
+
+    def send(name, source, target, device):
+        sender = used[0] % send_sem.shape[0]
+        used[0] += 1
+        if sender in in_flight:
+            in_flight[sender].wait_send()
+        copy = descriptor(source, target, device, sender, name)
         copy.start()
-        started.append(copy)
-        return copy
-
-    my_chunk = pl.ds(pl.multiple_of(group * chunk, chunk), chunk)
-    keep = pltpu.make_async_copy(xs_ref.at[my_chunk], rows.at[0, own], load_sem.at[4])
-    keep.start()
-    tail = pl.ds(row_count - WINDOW, WINDOW)
-    halo = [
-        send(source.at[:, tail], target.at[:, pl.ds(0, WINDOW)], next_dev)
-        for source, target in ((k_ref, k_ext), (v_ref, v_ext))
-    ]
-    z_out = [keep]
-    for step in range(1, groups):
-        plane = (group + step) % groups
-        there = pl.ds(pl.multiple_of(plane * chunk, chunk), chunk)
-        z_out.append(send(xs_ref.at[there], rows.at[step, own], (plane * 2 + member, tp)))
-    k_ext[:, pl.ds(WINDOW, row_count)] = k_ref[...]
-    v_ext[:, pl.ds(WINDOW, row_count)] = v_ref[...]
-
-    held = [dict() for _ in range(groups)]
-
-    def stage_a(s):
+        in_flight[sender] = copy
+
+    def receive(name, target, scope=None):
+        with NS(scope or "w" + name):
+            descriptor(target, target, x_dev, 0, name).wait_recv()
+
+    my_start = pl.multiple_of(group * chunk, chunk)
+    units = UNITS(chunk)
+    piece_rows = 16
+    near_pair = pl.ds(mine + member * 2, 2)
+    far_pair = pl.ds(mine + (1 - member) * 2, 2)
+    width_half = depth // 2
+    sides = (pl.ds(0, width_half), pl.ds(width_half, width_half))
+
+    def span_of(u):
+        return pl.ds(units[u][1], units[u][2])
+
+    def own_rows(s, begin, count):
+        if s == 0:
+            return xs_ref.at[pl.ds(pl.multiple_of(my_start + begin, piece_rows), count)]
+        return rows.at[s, own, pl.ds(begin, count)]
+
+    def depart(u):
+        s, begin, count = units[u]
         if s:
-            z_out[s].wait_recv()
-        else:
-            keep.wait()
-        held[s]["x"] = send(rows.at[s, own], rows.at[s, own], x_dev)
-        held[s]["y"] = send(rows.at[s, own], rows.at[s, own], y_dev)
-
-    def stage_b(s):
-        held[s]["x"].wait_recv()
-        held[s]["to_y"] = send(rows.at[s, slot_x], rows.at[s, slot_x], y_dev)
-
-    def stage_c(s):
-        held[s]["y"].wait_recv()
-        held[s]["to_y"].wait_recv()
-        held[s]["core"] = send(rows.at[s, mine_slots], rows.at[s, mine_slots], c_dev)
-
-    def stage_d(s):
-        held[s]["core"].wait_recv()
-        batch = 8 * chunk
-        tokens = rows[s, :, :, :depth].reshape(batch, depth)
-        shares = rows[s, :, :, depth:].reshape(batch, LANES).astype(jnp.float32)
-        lane = lax.broadcasted_iota(jnp.int32, shares.shape, 1) % (LANES // 2)
-
-        def one(e, carry):
+            there = pl.ds(pl.multiple_of(plane(s) * chunk + begin, piece_rows), count)
+            send(f"z{u}", xs_ref.at[there], rows.at[s, own, span_of(u)], (plane(s) * 2 + member, tp))
+
+    def arrive(u):
+        s = units[u][0]
+        receive(f"z{u}", rows.at[s, own, span_of(u)])
+
+    def gather_x(u):
+        s, begin, count = units[u]
+        for i in range(count // piece_rows):
+            at = begin + i * piece_rows
+            target = rows.at[s, own, pl.ds(at, piece_rows)]
+            send(f"x{u}{i}", own_rows(s, at, piece_rows), target, x_dev)
+
+    def gather_y(u):
+        s, begin, count = units[u]
+        send(f"y{u}", own_rows(s, begin, count), rows.at[s, own, span_of(u)], y_dev)
+
+    def relay(u, i):
+        s, begin, count = units[u]
+        block_at = rows.at[s, slot_x, pl.ds(begin + i * piece_rows, piece_rows)]
+        receive(f"x{u}{i}", block_at)
+        send(f"y{u}", block_at, block_at, y_dev)
+
+    def core_near(u):
+        s = units[u][0]
+        pair = rows.at[s, near_pair, span_of(u)]
+        send(f"core{u}", pair, pair, c_dev)
+
+    def core_far(u):
+        s = units[u][0]
+        pair = rows.at[s, far_pair, span_of(u)]
+        receive(f"y{u}", pair)
+        send(f"core{u}", pair, pair, c_dev)
+
+    def up(u, e):
+        s, begin, count = units[u]
+        if e == 0:
+            receive(f"core{u}", rows.at[s, other_slots, span_of(u)])
+        batch = 8 * count
+        with NS(f"up{u}{e}"):
+            tokens = rows[s, :, begin : begin + count, :depth].reshape(batch, depth)
+            shares = rows[s, :, begin : begin + count, depth:].reshape(batch, LANES)
+            lane = lax.broadcasted_iota(jnp.int32, shares.shape, 1) % (LANES // 2)
+            wanted = lane == member * wg.shape[0] + e
             share = jnp.sum(
-                jnp.where(lane == member * wg.shape[0] + e, shares, 0.0), axis=1, keepdims=True
+                jnp.where(wanted, shares.astype(jnp.float32), 0.0), axis=1, keepdims=True
             )
             pre = jnp.dot(tokens, wg[e], preferred_element_type=jnp.float32)
-            up = jnp.dot(tokens, wu[e], preferred_element_type=jnp.float32)
-            act[e] = (jax.nn.silu(pre) * up * share).astype(jnp.bfloat16)
-            return carry
-
-        lax.fori_loop(0, wg.shape[0], one, 0)
-        acts = jnp.concatenate([act[e] for e in range(wg.shape[0])], axis=1)
+            high = jnp.dot(tokens, wu[e], preferred_element_type=jnp.float32)
+            act[e, :batch] = (jax.nn.silu(pre) * high * share).astype(jnp.bfloat16)
+
+    def down(u):
+        s, begin, count = units[u]
+        batch = 8 * count
         tile = 512
+        acts = jnp.concatenate([act[e, :batch] for e in range(wg.shape[0])], axis=1)
 
         def column(n, carry):
             columns = pl.ds(pl.multiple_of(n * tile, tile), tile)
             value = jnp.dot(acts, wd[:, columns], preferred_element_type=jnp.float32)
-            part[s, :, :, columns] = value.astype(jnp.bfloat16).reshape(8, chunk, tile)
+            part[s, :, begin : begin + count, columns] = value.astype(jnp.bfloat16).reshape(
+                8, count, tile
+            )
             return carry
 
-        lax.fori_loop(0, depth // tile, column, 0)
-        held[s]["sum"] = send(part.at[s, other_slots], from_core.at[s], c_dev)
+        with NS(f"down{u}"):
+            for i, side in enumerate(sides):
+                tiles = width_half // tile
+                lax.fori_loop(i * tiles, (i + 1) * tiles, column, 0)
+                send(
+                    f"sum{u}",
+                    part.at[s, other_slots, span_of(u), side],
+                    from_core.at[s, :, span_of(u), side],
+                    c_dev,
+                )
+
+    def experts(u):
+        for e in range(wg.shape[0]):
+            up(u, e)
+        down(u)
 
     def add(index, term):
         part[index] = (part[index].astype(jnp.float32) + term.astype(jnp.float32)).astype(
             jnp.bfloat16
         )
 
-    def stage_e(s):
-        held[s]["sum"].wait_recv()
-        add((s, mine_slots), from_core[s])
-        held[s]["d_y"] = send(part.at[s, slot_d, lo], relay_y.at[s], y_dev)
-        held[s]["d_x"] = send(part.at[s, slot_d, hi], relay_x.at[s], x_dev)
-        held[s]["x_hi"] = send(part.at[s, slot_x, hi], from_x.at[s, hi], x_dev)
-        held[s]["y_lo"] = send(part.at[s, slot_y, lo], from_y.at[s, lo], y_dev)
-
-    def stage_f(s):
-        held[s]["d_y"].wait_recv()
-        add((s, slot_x, lo), relay_y[s])
-        held[s]["x_lo"] = send(part.at[s, slot_x, lo], from_x.at[s, lo], x_dev)
-        held[s]["d_x"].wait_recv()
-        add((s, slot_y, hi), relay_x[s])
-        held[s]["y_hi"] = send(part.at[s, slot_y, hi], from_y.at[s, hi], y_dev)
-
-    def stage_h(s):
-        for name in ("x_hi", "y_lo", "x_lo", "y_hi"):
-            held[s][name].wait_recv()
+    def scatter(u):
+        s, begin, count = units[u]
+        span = span_of(u)
+        left, right = sides
+        receive(f"sum{u}", from_core.at[s, :, span])
+        with NS(f"E{u}"):
+            add((s, mine_slots, span), from_core[s, :, span])
+        send(f"dy{u}", part.at[s, slot_d, span, left], relay_y.at[s, span], y_dev)
+        send(f"dx{u}", part.at[s, slot_d, span, right], relay_x.at[s, span], x_dev)
+        send(f"xy{u}", part.at[s, slot_x, span, right], from_xy.at[s, 0, span, right], x_dev)
+        send(f"xy{u}", part.at[s, slot_y, span, left], from_xy.at[s, 1, span, left], y_dev)
+
+    def scatter_relay(u):
+        s, begin, count = units[u]
+        span = span_of(u)
+        left, right = sides
+        receive(f"dy{u}", relay_y.at[s, span])
+        add((s, slot_x, span, left), relay_y[s, span])
+        send(f"xy{u}", part.at[s, slot_x, span, left], from_xy.at[s, 0, span, left], x_dev)
+        receive(f"dx{u}", relay_x.at[s, span])
+        add((s, slot_y, span, right), relay_x[s, span])
+        send(f"xy{u}", part.at[s, slot_y, span, right], from_xy.at[s, 1, span, right], y_dev)
+
+    def home(u):
+        s, begin, count = units[u]
+        span = span_of(u)
+        receive(f"xy{u}", from_xy.at[s, :, span], f"wH{u}")
         summed = (
-            part[s, own].astype(jnp.float32)
-            + from_x[s].astype(jnp.float32)
-            + from_y[s].astype(jnp.float32)
+            part[s, own, span].astype(jnp.float32)
+            + from_xy[s, 0, span].astype(jnp.float32)
+            + from_xy[s, 1, span].astype(jnp.float32)
         ).astype(jnp.bfloat16)
+        there = pl.ds(pl.multiple_of(my_start + begin, piece_rows), count)
         if s:
-            total[s] = summed
-            plane = (group + groups - s) % groups
-            held[s]["home"] = send(total.at[s], back.at[my_chunk], (plane * 2 + member, tp))
+            total[s, span] = summed
+            to = (group + groups - s) % groups
+            send(f"home{u}", total.at[s, span], back.at[there], (to * 2 + member, tp))
         else:
-            back[my_chunk] = summed
+            back[there] = summed
+
+    def settle(u):
+        s, begin, count = units[u]
+        if s:
+            there = pl.ds(pl.multiple_of(plane(s) * chunk + begin, piece_rows), count)
+            receive(f"home{u}", back.at[there])
 
     head_count = q_ref.shape[1] // HD
     query_at = lax.broadcasted_iota(jnp.int32, (WINDOW, 2 * WINDOW), 0)
@@ -336,76 +441,161 @@
         heads[tp, pl.ds(start, WINDOW)] = jnp.concatenate(outs, axis=1).astype(jnp.bfloat16)
         return carry
 
+    def att(first_block, last_block):
+        with NS(f"att{first_block}"):
+            lax.fori_loop(first_block, last_block, attend, 0)
+
     blocks = row_count // WINDOW
-    piece = row_count // 4
-    att_x = []
+    pieces = 4
+    piece = row_count // pieces
+    per = blocks // pieces
 
     def send_heads(i):
         span = pl.ds(i * piece, piece)
-        att_x.append(send(heads.at[tp, span], heads.at[tp, span], x_dev))
-
-    stage_a(0)
-    lax.fori_loop(1, blocks // 2, attend, 0)
-    stage_b(0)
-    stage_a(1)
-    lax.fori_loop(blocks // 2, blocks, attend, 0)
-    stage_c(0)
-    stage_b(1)
-    stage_a(2)
-    for copy in halo:
-        copy.wait_recv()
-    lax.fori_loop(0, 1, attend, 0)
+        send("heads_x", heads.at[tp, span], heads.at[tp, span], x_dev)
+
+    def share_heads():
+        send("heads_c", heads.at[tp], heads.at[tp], c_dev)
+
+    def relay_heads():
+        receive("heads_x", heads.at[tp_x])
+        send("heads_cx", heads.at[tp_x], heads.at[tp_x], c_dev)
+
+    def await_heads():
+        receive("heads_c", heads.at[tp_c])
+        receive("heads_cx", heads.at[tp_c])
+
+    written = []
+
+    def project(i):
+        span = pl.ds(i * piece, piece)
+        with NS(f"proj{i}"):
+            joined = jnp.concatenate([heads[t, span] for t in range(4)], axis=1)
+            mixed[span] = jnp.dot(joined, proj[...], preferred_element_type=jnp.float32).astype(
+                jnp.bfloat16
+            )
+        copy = pltpu.make_async_copy(mixed.at[span], mixer_hbm.at[span], out_sem.at[1 + i])
+        copy.start()
+        written.append(copy)
+
+    with NS("wqkv"):
+        for load in middle:
+            load.wait()
+    for name, ext in (("k", k_ext), ("v", v_ext)):
+        send(name, ext.at[:, pl.ds(row_count, WINDOW)], ext.at[:, pl.ds(0, WINDOW)], next_dev)
+    gather_x(FIRST)
+    gather_y(FIRST)
+    depart("1")
+    keep = pltpu.make_async_copy(
+        xs_ref.at[pl.ds(my_start, chunk)], rows.at[0, own], out_sem.at[0]
+    )
+    keep.start()
+
+    def take_halo():
+        for name, ext in (("k", k_ext), ("v", v_ext)):
+            receive(name, ext.at[:, pl.ds(0, WINDOW)])
+
+    def take_weights():
+        with NS("loads"):
+            for load in late:
+                load.wait()
+
+    att(2, 4)
+    send_heads(1)
+    att(4, 6)
+    depart("2")
+    relay("0", 0)
+    relay("0", 1)
+    att(6, 7)
+    arrive("1")
+    gather_x("1")
+    gather_y("1")
+    att(7, 8)
+    att(1, 2)
+    take_halo()
+    depart("a")
+    depart("b")
+    att(0, 1)
+    share_heads()
+    take_weights()
+    keep.wait()
+    core_near("0")
+    arrive("2")
+    gather_x("2")
+    core_far("0")
+    relay("1", 0)
+    relay("1", 1)
+    gather_y("2")
+    core_near("1")
+    arrive("a")
+    gather_x("a")
+    arrive("b")
+    gather_x("b")
+    up("0", 0)
+    up("0", 1)
+    relay("2", 0)
+    send_heads(2)
+    send_heads(3)
     send_heads(0)
-    att_c = send(heads.at[tp], heads.at[tp], c_dev)
-    for load in loads:
-        load.wait()
-    stage_d(0)
-    stage_c(1)
-    stage_b(2)
-    stage_a(3)
-    stage_e(0)
-    stage_d(1)
-    send_heads(1)
-    stage_f(0)
-    stage_c(2)
-    stage_b(3)
-    stage_e(1)
-    stage_d(2)
-    stage_h(0)
-    send_heads(2)
-    stage_f(1)
-    stage_c(3)
-    stage_e(2)
-    stage_d(3)
-    stage_h(1)
-    stage_f(2)
-    stage_e(3)
-    send_heads(3)
-    stage_h(2)
-    stage_f(3)
-    for copy in att_x:
-        copy.wait_recv()
-    att_cx = send(heads.at[tp_x], heads.at[tp_x], c_dev)
-    att_c.wait_recv()
-    att_cx.wait_recv()
-    stage_h(3)
-
-    def project(i, carry):
-        span = pl.ds(pl.multiple_of(i * piece, piece), piece)
-        joined = jnp.concatenate([heads[t, span] for t in range(4)], axis=1)
-        mixer_ref[span] = jnp.dot(joined, proj[...], preferred_element_type=jnp.float32).astype(
-            jnp.bfloat16
-        )
-        return carry
-
-    lax.fori_loop(0, 4, project, 0)
-    for s in range(1, groups):
-        held[s]["home"].wait_recv()
-    out_ref[...] = lax.dot_general(
-        take, back[...], (((0,), (0,)), ((), ())), preferred_element_type=jnp.float32
-    ).astype(jnp.bfloat16)
-    for copy in started:
-        copy.wait_send()
+    down("0")
+    relay("2", 1)
+    gather_y("a")
+    core_near("2")
+    core_far("1")
+    relay("a", 0)
+    gather_y("b")
+    core_near("a")
+    relay("b", 0)
+    core_near("b")
+    up("1", 0)
+    up("1", 1)
+    down("1")
+    core_far("2")
+    scatter("1")
+    up("2", 0)
+    up("2", 1)
+    core_far("a")
+    down("2")
+    core_far("b")
+    scatter("2")
+    relay_heads()
+    scatter_relay("1")
+    experts("a")
+    scatter_relay("2")
+    experts("b")
+    scatter("a")
+    home("1")
+    scatter("b")
+    home("2")
+    scatter_relay("a")
+    scatter("0")
+    await_heads()
+    project(0)
+    scatter_relay("b")
+    home("a")
+    project(1)
+    scatter_relay("0")
+    home("b")
+    project(2)
+    project(3)
+    home("0")
+    settle("1")
+    settle("2")
+    settle("a")
+    settle("b")
+    with NS("finish"):
+        moved[...] = lax.dot_general(
+            take, back[...], (((0,), (0,)), ((), ())), preferred_element_type=jnp.float32
+        ).astype(jnp.bfloat16)
+    copy = pltpu.make_async_copy(moved, out_hbm, out_sem.at[1 + pieces])
+    copy.start()
+    written.append(copy)
+    with NS("wsend"):
+        for copy in in_flight.values():
+            copy.wait_send()
+    with NS("wout"):
+        for copy in written:
+            copy.wait()
 
 
 def fused(
@@ -430,19 +620,23 @@
     row_count, head_width = q_heads.shape
     down = expert_down.reshape(experts * hidden, depth)
     chunk = block // groups
-    copies = 14 * groups + 8
     bf16 = jnp.bfloat16
     anywhere = pl.BlockSpec(memory_space=pl.ANY)
-    vmem = pl.BlockSpec(memory_space=pltpu.VMEM)
     return pl.pallas_call(
         functools.partial(fused_kernel, groups),
         out_shape=(
             jax.ShapeDtypeStruct((row_count, proj.shape[1]), bf16),
             jax.ShapeDtypeStruct((block, depth), bf16),
         ),
-        in_specs=[pl.BlockSpec(memory_space=pltpu.SMEM)] + [vmem] * 7 + [anywhere] * 5,
-        out_specs=(vmem, vmem),
+        in_specs=[anywhere] * 13,
+        out_specs=(anywhere, anywhere),
         scratch_shapes=[
+            pltpu.SMEM(sinks.shape, jnp.float32),
+            pltpu.VMEM(q_heads.shape, bf16),
+            pltpu.VMEM((1, depth), jnp.float32),
+            pltpu.VMEM((groups, depth), bf16),
+            pltpu.VMEM((router_expert.shape[1], depth), bf16),
+            pltpu.VMEM((2, block), jnp.int32),
             pltpu.VMEM((HD, row_count + WINDOW), bf16),
             pltpu.VMEM((HD, row_count + WINDOW), bf16),
             pltpu.VMEM((block, depth), bf16),
@@ -456,15 +650,17 @@
             pltpu.VMEM(proj.shape, bf16),
             pltpu.VMEM((experts, 8 * chunk, hidden), bf16),
             pltpu.VMEM((groups, 4, chunk, depth), bf16),
-            pltpu.VMEM((groups, chunk // 2, depth), bf16),
-            pltpu.VMEM((groups, chunk // 2, depth), bf16),
-            pltpu.VMEM((groups, chunk, depth), bf16),
-            pltpu.VMEM((groups, chunk, depth), bf16),
+            pltpu.VMEM((groups, chunk, depth // 2), bf16),
+            pltpu.VMEM((groups, chunk, depth // 2), bf16),
+            pltpu.VMEM((groups, 2, chunk, depth), bf16),
             pltpu.VMEM((groups, chunk, depth), bf16),
             pltpu.VMEM((block, depth), bf16),
+            pltpu.VMEM((row_count, proj.shape[1]), bf16),
+            pltpu.VMEM((block, depth), bf16),
+            pltpu.SemaphoreType.DMA((13,)),
             pltpu.SemaphoreType.DMA((6,)),
-            pltpu.SemaphoreType.DMA((copies,)),
-            pltpu.SemaphoreType.DMA((copies,)),
+            pltpu.SemaphoreType.DMA((SENDERS,)),
+            pltpu.SemaphoreType.DMA((RECEIVERS,)),
         ],
         cost_estimate=pl.CostEstimate(
             flops=20_000_000_000, bytes_accessed=20_000_000, transcendentals=0

time: 69.1 us -> 63.4 us (0.918)
  Pallas kernels: 65.1 us -> 59.4 us
    pallas_call x1, Pallas kernels: 65.1 us -> 59.4 us  [fused(): pl.pallas_call(functools.partial(fused_kernel, groups), out_shape=(jax.Sh...]
where the time goes in v1:
time: 63.4 us; the launch traced here: 63.2 us
  Pallas kernels  59.4 us (94%)
  local copies, waits for them, and re-layouts  3.12 us (5%)
  between operations  0.65 us (1%)
    pallas_call x1, Pallas kernels, fused(): pl.pallas_call(functools.partial(fused_kernel, groups), out_shape=(jax.Sh...  59.4 us
    unnamed x4, local copies, waits for them, and re-layouts  3.12 us

profile of v1, /device:TPU:0, one launch (start us, length us, event | category | flops | bytes accessed | tf_op | source)
XLA Modules:
  0.0 63.2 jit_solution(16879737152859686686)
XLA Ops:
  0.6 59.4 %shard_map.140 = (bf16[1024,512]{1,0:T(8,128)(2,1)}, bf16[128,2048]{1,0:T(8,128)(2,1)}) custom-call(f32[4]{0:T(128)} %sink_hbm.1, bf16[1024,256]{1,0:T(8,128)(2,1)} %q_hbm.1, bf16[64,1024]{1,0:T(8,128)(2,1)} %bitcast.8, bf16[64,1024]{1,0:T(8,128)(2,1)} %bitcast.9, f32[1,2048]{1,0:T(1,128)} %bitcast.12, bf16[4,2048]{1,0:T(4,128)(2,1)} %bitcast.11, ...), custom_call_target="tpu_custom_call" | custom-call | flops 20000000000 | bytes 20000000 | tf_op jit(solution)/shard_map/pallas_call | solution.py:625
  60.1 0.0 copy-start
  60.1 2.3 %copy.17 = bf16[1024,512]{1,0:T(8,128)(2,1)} copy(bf16[1024,512]{1,0:T(8,128)(2,1)} %get-tuple-element.4) | data formatting | bytes 2097152
  62.4 0.0 copy-done
  62.4 0.8 %copy.18 = bf16[128,2048]{1,0:T(8,128)(2,1)} copy(bf16[128,2048]{1,0:T(8,128)(2,1)S(1)} %copy-done) | data formatting | bytes 1048576
Async XLA Ops:
  60.1 2.3 %copy-start = (bf16[128,2048]{1,0:T(8,128)(2,1)S(1)}, bf16[128,2048]{1,0:T(8,128)(2,1)}, u32[]{:S(2)}) copy-start(bf16[128,2048]{1,0:T(8,128)(2,1)} %get-tuple-element.5) | copy-start | bytes 1572868

commit v2 on v1

--- a/solution.py
+++ b/solution.py
@@ -1,3 +1,4 @@
+import contextlib
 import functools
 
 import jax
@@ -62,10 +63,17 @@
 
 LANES = 128
 MESH = pl.DeviceIdType.MESH
-NS = jax.named_scope
+
+
+@contextlib.contextmanager
+def NS(name):
+    pl.delay(1)
+    yield
+    pl.delay(1)
+
 FIRST = "0"
 SENDERS = 24
-RECEIVERS = 52
+RECEIVERS = 51
 
 
 def UNITS(chunk):
@@ -94,8 +102,8 @@
     up_hbm,
     down_hbm,
     proj_hbm,
-    mixer_hbm,
-    out_hbm,
+    mixed,
+    moved,
     sink_ref,
     q_ref,
     gain_ref,
@@ -120,8 +128,6 @@
     from_xy,
     total,
     back,
-    mixed,
-    moved,
     load_sem,
     out_sem,
     send_sem,
@@ -370,6 +376,10 @@
         )
 
     def scatter(u):
+        scatter_far(u)
+        scatter_near(u)
+
+    def scatter_far(u):
         s, begin, count = units[u]
         span = span_of(u)
         left, right = sides
@@ -378,6 +388,11 @@
             add((s, mine_slots, span), from_core[s, :, span])
         send(f"dy{u}", part.at[s, slot_d, span, left], relay_y.at[s, span], y_dev)
         send(f"dx{u}", part.at[s, slot_d, span, right], relay_x.at[s, span], x_dev)
+
+    def scatter_near(u):
+        s, begin, count = units[u]
+        span = span_of(u)
+        left, right = sides
         send(f"xy{u}", part.at[s, slot_x, span, right], from_xy.at[s, 0, span, right], x_dev)
         send(f"xy{u}", part.at[s, slot_y, span, left], from_xy.at[s, 1, span, left], y_dev)
 
@@ -465,8 +480,6 @@
         receive("heads_c", heads.at[tp_c])
         receive("heads_cx", heads.at[tp_c])
 
-    written = []
-
     def project(i):
         span = pl.ds(i * piece, piece)
         with NS(f"proj{i}"):
@@ -474,9 +487,6 @@
             mixed[span] = jnp.dot(joined, proj[...], preferred_element_type=jnp.float32).astype(
                 jnp.bfloat16
             )
-        copy = pltpu.make_async_copy(mixed.at[span], mixer_hbm.at[span], out_sem.at[1 + i])
-        copy.start()
-        written.append(copy)
 
     with NS("wqkv"):
         for load in middle:
@@ -513,42 +523,42 @@
     att(7, 8)
     att(1, 2)
     take_halo()
-    depart("a")
-    depart("b")
     att(0, 1)
     share_heads()
     take_weights()
     keep.wait()
     core_near("0")
-    arrive("2")
-    gather_x("2")
     core_far("0")
     relay("1", 0)
     relay("1", 1)
+    depart("a")
+    depart("b")
+    core_near("1")
+    arrive("2")
+    gather_x("2")
     gather_y("2")
-    core_near("1")
-    arrive("a")
-    gather_x("a")
-    arrive("b")
-    gather_x("b")
+    send_heads(2)
     up("0", 0)
     up("0", 1)
     relay("2", 0)
-    send_heads(2)
+    relay("2", 1)
+    core_near("2")
+    arrive("a")
+    gather_x("a")
+    gather_y("a")
+    arrive("b")
+    gather_x("b")
+    gather_y("b")
     send_heads(3)
     send_heads(0)
+    core_far("1")
     down("0")
-    relay("2", 1)
-    gather_y("a")
-    core_near("2")
-    core_far("1")
+    up("1", 0)
     relay("a", 0)
-    gather_y("b")
     core_near("a")
+    up("1", 1)
     relay("b", 0)
     core_near("b")
-    up("1", 0)
-    up("1", 1)
     down("1")
     core_far("2")
     scatter("1")
@@ -557,26 +567,27 @@
     core_far("a")
     down("2")
     core_far("b")
+    scatter_relay("1")
     scatter("2")
     relay_heads()
-    scatter_relay("1")
     experts("a")
-    scatter_relay("2")
     experts("b")
     scatter("a")
+    scatter_relay("2")
     home("1")
     scatter("b")
+    scatter_relay("a")
+    scatter_far("0")
+    await_heads()
     home("2")
-    scatter_relay("a")
-    scatter("0")
-    await_heads()
     project(0)
     scatter_relay("b")
+    scatter_near("0")
     home("a")
     project(1)
     scatter_relay("0")
+    project(2)
     home("b")
-    project(2)
     project(3)
     home("0")
     settle("1")
@@ -587,15 +598,32 @@
         moved[...] = lax.dot_general(
             take, back[...], (((0,), (0,)), ((), ())), preferred_element_type=jnp.float32
         ).astype(jnp.bfloat16)
-    copy = pltpu.make_async_copy(moved, out_hbm, out_sem.at[1 + pieces])
-    copy.start()
-    written.append(copy)
     with NS("wsend"):
         for copy in in_flight.values():
             copy.wait_send()
-    with NS("wout"):
-        for copy in written:
-            copy.wait()
+
+
+def store_kernel(mixed, moved, mixer_hbm, out_hbm, sem):
+    copies = [
+        pltpu.make_async_copy(source, target, sem.at[i])
+        for i, (source, target) in enumerate(((mixed, mixer_hbm), (moved, out_hbm)))
+    ]
+    for copy in copies:
+        copy.start()
+    for copy in copies:
+        copy.wait()
+
+
+def store(mixed, moved):
+    anywhere = pl.BlockSpec(memory_space=pl.ANY)
+    return pl.pallas_call(
+        store_kernel,
+        out_shape=tuple(jax.ShapeDtypeStruct(v.shape, v.dtype) for v in (mixed, moved)),
+        in_specs=[anywhere] * 2,
+        out_specs=(anywhere, anywhere),
+        scratch_shapes=[pltpu.SemaphoreType.DMA((2,))],
+        compiler_params=pltpu.CompilerParams(vmem_limit_bytes=2**20),
+    )(*(pltpu.with_memory_space_constraint(v, pltpu.VMEM) for v in (mixed, moved)))
 
 
 def fused(
@@ -622,14 +650,14 @@
     chunk = block // groups
     bf16 = jnp.bfloat16
     anywhere = pl.BlockSpec(memory_space=pl.ANY)
-    return pl.pallas_call(
+    mixed, moved = pl.pallas_call(
         functools.partial(fused_kernel, groups),
         out_shape=(
-            jax.ShapeDtypeStruct((row_count, proj.shape[1]), bf16),
-            jax.ShapeDtypeStruct((block, depth), bf16),
+            pltpu.VMEM((row_count, proj.shape[1]), bf16),
+            pltpu.VMEM((block, depth), bf16),
         ),
         in_specs=[anywhere] * 13,
-        out_specs=(anywhere, anywhere),
+        out_specs=(pl.BlockSpec(memory_space=pltpu.VMEM),) * 2,
         scratch_shapes=[
             pltpu.SMEM(sinks.shape, jnp.float32),
             pltpu.VMEM(q_heads.shape, bf16),
@@ -655,10 +683,8 @@
             pltpu.VMEM((groups, 2, chunk, depth), bf16),
             pltpu.VMEM((groups, chunk, depth), bf16),
             pltpu.VMEM((block, depth), bf16),
-            pltpu.VMEM((row_count, proj.shape[1]), bf16),
-            pltpu.VMEM((block, depth), bf16),
             pltpu.SemaphoreType.DMA((13,)),
-            pltpu.SemaphoreType.DMA((6,)),
+            pltpu.SemaphoreType.DMA((1,)),
             pltpu.SemaphoreType.DMA((SENDERS,)),
             pltpu.SemaphoreType.DMA((RECEIVERS,)),
         ],
@@ -666,23 +692,29 @@
             flops=20_000_000_000, bytes_accessed=20_000_000, transcendentals=0
         ),
         compiler_params=pltpu.CompilerParams(
-            collective_id=0, has_side_effects=True, vmem_limit_bytes=56 * 2**20
+            collective_id=0, has_side_effects=True, vmem_limit_bytes=40 * 2**20
         ),
     )(
-        sinks,
-        q_heads,
-        k_heads.T,
-        v_heads.T,
-        gain[None, :],
-        router_group.T,
-        router_expert.T,
-        routes.T,
-        tokens_b,
-        expert_gate,
-        expert_up,
-        down,
-        proj,
-    )
+        *(
+            pltpu.with_memory_space_constraint(value, pltpu.HBM)
+            for value in (
+                sinks,
+                q_heads,
+                k_heads.T,
+                v_heads.T,
+                gain[None, :],
+                router_group.T,
+                router_expert.T,
+                routes.T,
+                tokens_b,
+                expert_gate,
+                expert_up,
+                down,
+                proj,
+            )
+        )
+    )
+    return store(mixed, moved)
 
 
 def per_device(

time: 63.4 us -> 56.1 us (0.88)
  Pallas kernels: 59.4 us -> 55.3 us
  local copies, waits for them, and re-layouts: 3.12 us -> 0 us
    pallas_call x1 -> x2, Pallas kernels: 59.4 us -> 55.3 us  [the longest x1 54.1 us: fused(): pl.pallas_call(functools.partial(fused_kernel, groups), out_shape=(pltpu....]
    unnamed x4 -> x0, local copies, waits for them, and re-layouts: 3.12 us -> none
where the time goes in v2:
time: 56.1 us; the launch traced here: 55.9 us
  Pallas kernels  55.3 us (99%)
  between operations  0.64 us (1%)
    pallas_call x1, Pallas kernels, fused(): pl.pallas_call(functools.partial(fused_kernel, groups), out_shape=(pltpu....  54.1 us
    pallas_call x1, Pallas kernels, store(): pl.pallas_call(store_kernel, out_shape=tuple((jax.ShapeDtypeStruct(v.shap...  1.16 us

profile of v2, /device:TPU:0, one launch (start us, length us, event | category | flops | bytes accessed | tf_op | source)
XLA Modules:
  0.0 55.9 jit_solution(13732693546634837357)
XLA Ops:
  0.6 54.1 %shard_map.140 = (bf16[1024,512]{1,0:T(8,128)(2,1)S(1)}, bf16[128,2048]{1,0:T(8,128)(2,1)S(1)}) custom-call(f32[4]{0:T(128)} %sink_hbm.1, bf16[1024,256]{1,0:T(8,128)(2,1)} %q_hbm.1, bf16[64,1024]{1,0:T(8,128)(2,1)} %bitcast.8, bf16[64,1024]{1,0:T(8,128)(2,1)} %bitcast.9, f32[1,2048]{1,0:T(1,128)} %bitcast.12, bf16[4,2048]{1,0:T(4,128)(2,1)} %bitcast.11, ...), custom_call_target="tpu_custom_call" | custom-call | flops 20000000000 | bytes 20000000 | tf_op jit(solution)/shard_map/pallas_call | solution.py:653
  54.8 1.2 %shard_map.141 = (bf16[1024,512]{1,0:T(8,128)(2,1)}, bf16[128,2048]{1,0:T(8,128)(2,1)}) custom-call(bf16[1024,512]{1,0:T(8,128)(2,1)S(1)} %get-tuple-element.4.mixed, bf16[128,2048]{1,0:T(8,128)(2,1)S(1)} %get-tuple-element.5.moved), custom_call_target="tpu_custom_call" | custom-call | tf_op jit(solution)/shard_map/pallas_call | solution.py:619

commit v3 on v2

--- a/solution.py
+++ b/solution.py
@@ -73,7 +73,7 @@
 
 FIRST = "0"
 SENDERS = 24
-RECEIVERS = 51
+RECEIVERS = 58
 
 
 def UNITS(chunk):
@@ -81,7 +81,8 @@
     return {
         "0": (0, 0, chunk),
         "1": (1, 0, chunk),
-        "2": (2, 0, chunk),
+        "c": (2, 0, half),
+        "d": (2, half, half),
         "a": (3, 0, half),
         "b": (3, half, half),
     }
@@ -103,7 +104,8 @@
     down_hbm,
     proj_hbm,
     mixed,
-    moved,
+    back,
+    take_out,
     sink_ref,
     q_ref,
     gain_ref,
@@ -114,6 +116,7 @@
     v_ext,
     tokens,
     xs_ref,
+    share_ref,
     heads,
     rows,
     part,
@@ -127,7 +130,6 @@
     relay_y,
     from_xy,
     total,
-    back,
     load_sem,
     out_sem,
     send_sem,
@@ -139,7 +141,7 @@
     tp_x, tp_c = (1 - x) * 2 + core, x * 2 + (1 - core)
     ep_y = group * 2 + (1 - member)
     ep_count = groups * 2
-    x_dev, y_dev, c_dev = (ep, tp_x), (ep_y, tp), (ep, tp_c)
+    x_dev, y_dev, c_dev, d_dev = (ep, tp_x), (ep_y, tp), (ep, tp_c), (ep_y, tp_x)
     next_dev = ((ep + 1) % ep_count, tp)
     prev_dev = ((ep + ep_count - 1) % ep_count, tp)
     depth = back.shape[1]
@@ -158,7 +160,7 @@
 
     barrier = pltpu.get_barrier_semaphore()
     ahead = [plane(step) * 2 + member for step in range(1, groups)]
-    peers = [(there, tp) for there in ahead] + [x_dev, y_dev, c_dev, next_dev, prev_dev]
+    peers = [(there, tp) for there in ahead] + [x_dev, y_dev, c_dev, d_dev, next_dev, prev_dev]
     for peer in peers:
         pl.semaphore_signal(barrier, inc=1, device_id=peer, device_id_type=MESH)
 
@@ -186,8 +188,24 @@
     early, middle, late = loads[:5], loads[5:9], loads[9:]
     for load in early + middle:
         load.start()
+    early[4].wait()
+    routes = route_ref[...]
+    route_a, route_b = routes[0:1], routes[1:2]
+    group_experts = expert_ref.shape[0] // groups
+    group_at = lax.broadcasted_iota(jnp.int32, (groups, block), 0)
+    inside = route_a - group_at * group_experts
+    named = (inside >= 0) & (inside < group_experts)
+    row_at = lax.broadcasted_iota(jnp.int32, (block, block), 0)
+    column_at = lax.broadcasted_iota(jnp.int32, (block, block), 1)
+    earlier = jnp.where(row_at < column_at, 1.0, 0.0).astype(jnp.bfloat16)
+    counts = jnp.dot(
+        jnp.where(named, 1.0, 0.0).astype(jnp.bfloat16), earlier, preferred_element_type=jnp.float32
+    )
+    first_row = (group_at * chunk).astype(jnp.float32)
+    place = jnp.sum(jnp.where(named, counts + first_row, 0.0), axis=0, keepdims=True)
+    take = jnp.where(row_at.astype(jnp.float32) == place, 1.0, 0.0).astype(jnp.bfloat16)
     with NS("wearly"):
-        for load in early:
+        for load in early[:4]:
             load.wait()
     for load in late:
         load.start()
@@ -195,51 +213,8 @@
     scale = lax.rsqrt(jnp.mean(values * values, axis=1, keepdims=True) + 1e-06)
     normed = (values * scale * gain_ref[...]).astype(jnp.bfloat16)
     across = (((1,), (1,)), ((), ()))
-    group_logits = lax.dot_general(
-        group_ref[...], normed, across, preferred_element_type=jnp.float32
-    )
-    expert_logits = lax.dot_general(
-        expert_ref[...], normed, across, preferred_element_type=jnp.float32
-    )
-    routes = route_ref[...]
-    route_a, route_b = routes[0:1], routes[1:2]
-    group_experts = expert_ref.shape[0] // groups
-    group_at = lax.broadcasted_iota(jnp.int32, (groups, block), 0)
-    inside = route_a - group_at * group_experts
-    named = (inside >= 0) & (inside < group_experts)
-    group_exp = jnp.exp(group_logits - jnp.max(group_logits, axis=0, keepdims=True))
-    group_share = jnp.sum(jnp.where(named, group_exp, 0.0), axis=0, keepdims=True) / jnp.sum(
-        group_exp, axis=0, keepdims=True
-    )
-    expert_at = lax.broadcasted_iota(jnp.int32, expert_logits.shape, 0)
-    logit_a = jnp.sum(jnp.where(expert_at == route_a, expert_logits, 0.0), axis=0, keepdims=True)
-    logit_b = jnp.sum(jnp.where(expert_at == route_b, expert_logits, 0.0), axis=0, keepdims=True)
-    top = jnp.maximum(logit_a, logit_b)
-    exp_a, exp_b = jnp.exp(logit_a - top), jnp.exp(logit_b - top)
-    gate_a = group_share * (exp_a / (exp_a + exp_b))
-    gate_b = group_share * (exp_b / (exp_a + exp_b))
-    base = jnp.sum(jnp.where(named, group_at * group_experts, 0), axis=0, keepdims=True)
-    lane_at = lax.broadcasted_iota(jnp.int32, (LANES // 2, block), 0)
-    share_t = jnp.where(lane_at == route_a - base, gate_a, 0.0) + jnp.where(
-        lane_at == route_b - base, gate_b, 0.0
-    )
-    coarse = share_t.astype(jnp.bfloat16)
-    fine = (share_t - coarse.astype(jnp.float32)).astype(jnp.bfloat16)
-    row_at = lax.broadcasted_iota(jnp.int32, (block, block), 0)
-    column_at = lax.broadcasted_iota(jnp.int32, (block, block), 1)
-    earlier = jnp.where(row_at < column_at, 1.0, 0.0).astype(jnp.bfloat16)
-    counts = jnp.dot(
-        jnp.where(named, 1.0, 0.0).astype(jnp.bfloat16), earlier, preferred_element_type=jnp.float32
-    )
-    first_row = (group_at * chunk).astype(jnp.float32)
-    place = jnp.sum(jnp.where(named, counts + first_row, 0.0), axis=0, keepdims=True)
-    take = jnp.where(row_at.astype(jnp.float32) == place, 1.0, 0.0).astype(jnp.bfloat16)
-    xs_ref[:, :depth] = jnp.dot(take, normed, preferred_element_type=jnp.float32).astype(
-        jnp.bfloat16
-    )
-    xs_ref[:, depth:] = lax.dot_general(
-        take, jnp.concatenate([coarse, fine], axis=0), across, preferred_element_type=jnp.float32
-    ).astype(jnp.bfloat16)
+    xs_ref[...] = jnp.dot(take, normed, preferred_element_type=jnp.float32).astype(jnp.bfloat16)
+    take_out[...] = take
     with NS("barrier"):
         pl.semaphore_wait(barrier, len(peers))
 
@@ -329,13 +304,17 @@
             receive(f"core{u}", rows.at[s, other_slots, span_of(u)])
         batch = 8 * count
         with NS(f"up{u}{e}"):
-            tokens = rows[s, :, begin : begin + count, :depth].reshape(batch, depth)
-            shares = rows[s, :, begin : begin + count, depth:].reshape(batch, LANES)
-            lane = lax.broadcasted_iota(jnp.int32, shares.shape, 1) % (LANES // 2)
-            wanted = lane == member * wg.shape[0] + e
+            tokens = rows[s, :, begin : begin + count].reshape(batch, depth)
+            held = share_ref[s].astype(jnp.float32)
+            at = lax.broadcasted_iota(jnp.int32, held.shape, 1) % group_experts
+            wanted = at == member * wg.shape[0] + e
+            by_lane = jnp.sum(jnp.where(wanted, held, 0.0), axis=1, keepdims=True)
+            shape = (8, count, block)
+            lane = lax.broadcasted_iota(jnp.int32, shape, 2) - group * chunk - begin
+            picked = lane == lax.broadcasted_iota(jnp.int32, shape, 1)
             share = jnp.sum(
-                jnp.where(wanted, shares.astype(jnp.float32), 0.0), axis=1, keepdims=True
-            )
+                jnp.where(picked, jnp.broadcast_to(by_lane, shape), 0.0), axis=2, keepdims=True
+            ).reshape(batch, 1)
             pre = jnp.dot(tokens, wg[e], preferred_element_type=jnp.float32)
             high = jnp.dot(tokens, wu[e], preferred_element_type=jnp.float32)
             act[e, :batch] = (jax.nn.silu(pre) * high * share).astype(jnp.bfloat16)
@@ -420,15 +399,12 @@
         if s:
             total[s, span] = summed
             to = (group + groups - s) % groups
-            send(f"home{u}", total.at[s, span], back.at[there], (to * 2 + member, tp))
+            send("home", total.at[s, span], back.at[there], (to * 2 + member, tp))
         else:
             back[there] = summed
 
-    def settle(u):
-        s, begin, count = units[u]
-        if s:
-            there = pl.ds(pl.multiple_of(plane(s) * chunk + begin, piece_rows), count)
-            receive(f"home{u}", back.at[there])
+    def settle():
+        receive("home", back.at[pl.ds(0, block - chunk)])
 
     head_count = q_ref.shape[1] // HD
     query_at = lax.broadcasted_iota(jnp.int32, (WINDOW, 2 * WINDOW), 0)
@@ -463,10 +439,9 @@
     blocks = row_count // WINDOW
     pieces = 4
     piece = row_count // pieces
-    per = blocks // pieces
-
-    def send_heads(i):
-        span = pl.ds(i * piece, piece)
+
+    def send_heads(begin, end):
+        span = pl.ds(begin * WINDOW, (end - begin) * WINDOW)
         send("heads_x", heads.at[tp, span], heads.at[tp, span], x_dev)
 
     def share_heads():
@@ -488,14 +463,60 @@
                 jnp.bfloat16
             )
 
+    gather_x(FIRST)
+    gather_y(FIRST)
+    depart("1")
+    group_logits = lax.dot_general(
+        group_ref[...], normed, across, preferred_element_type=jnp.float32
+    )
+    expert_logits = lax.dot_general(
+        expert_ref[...], normed, across, preferred_element_type=jnp.float32
+    )
+    group_exp = jnp.exp(group_logits - jnp.max(group_logits, axis=0, keepdims=True))
+    group_share = jnp.sum(jnp.where(named, group_exp, 0.0), axis=0, keepdims=True) / jnp.sum(
+        group_exp, axis=0, keepdims=True
+    )
+    expert_at = lax.broadcasted_iota(jnp.int32, expert_logits.shape, 0)
+    logit_a = jnp.sum(jnp.where(expert_at == route_a, expert_logits, 0.0), axis=0, keepdims=True)
+    logit_b = jnp.sum(jnp.where(expert_at == route_b, expert_logits, 0.0), axis=0, keepdims=True)
+    top = jnp.maximum(logit_a, logit_b)
+    exp_a, exp_b = jnp.exp(logit_a - top), jnp.exp(logit_b - top)
+    gate_a = group_share * (exp_a / (exp_a + exp_b))
+    gate_b = group_share * (exp_b / (exp_a + exp_b))
+    base = jnp.sum(jnp.where(named, group_at * group_experts, 0), axis=0, keepdims=True)
+    slot_at = lax.broadcasted_iota(jnp.int32, (group_experts, block), 0)
+    share_t = jnp.where(slot_at == route_a - base, gate_a, 0.0) + jnp.where(
+        slot_at == route_b - base, gate_b, 0.0
+    )
+    coarse = share_t.astype(jnp.bfloat16)
+    fine = (share_t - coarse.astype(jnp.float32)).astype(jnp.bfloat16)
+    for i, piece_of in enumerate((coarse, fine)):
+        share_ref[0, own, pl.ds(i * group_experts, group_experts)] = lax.dot_general(
+            piece_of, take, across, preferred_element_type=jnp.float32
+        ).astype(jnp.bfloat16)
+    for step in range(1, groups):
+        there = (plane(step) * 2 + member, tp)
+        send("share_z", share_ref.at[0, own], share_ref.at[step, own], there)
+
+    def spread_shares():
+        receive("share_z", share_ref.at[pl.ds(1, groups - 1), own])
+        mine_now = share_ref.at[:, own]
+        for device in (d_dev, x_dev, y_dev):
+            send("share", mine_now, mine_now, device)
+
+    def swap_shares():
+        receive("share", share_ref.at[:, pl.ds(mine, 3)])
+        core_now = share_ref.at[:, mine_slots]
+        send("share_c", core_now, core_now, c_dev)
+
+    def take_shares():
+        receive("share_c", share_ref.at[:, other_slots])
+
     with NS("wqkv"):
         for load in middle:
             load.wait()
     for name, ext in (("k", k_ext), ("v", v_ext)):
-        send(name, ext.at[:, pl.ds(row_count, WINDOW)], ext.at[:, pl.ds(0, WINDOW)], next_dev)
-    gather_x(FIRST)
-    gather_y(FIRST)
-    depart("1")
+        send("halo" + name, ext.at[:, pl.ds(row_count, WINDOW)], ext.at[:, pl.ds(0, WINDOW)], next_dev)
     keep = pltpu.make_async_copy(
         xs_ref.at[pl.ds(my_start, chunk)], rows.at[0, own], out_sem.at[0]
     )
@@ -503,7 +524,7 @@
 
     def take_halo():
         for name, ext in (("k", k_ext), ("v", v_ext)):
-            receive(name, ext.at[:, pl.ds(0, WINDOW)])
+            receive("halo" + name, ext.at[:, pl.ds(0, WINDOW)])
 
     def take_weights():
         with NS("loads"):
@@ -511,12 +532,14 @@
                 load.wait()
 
     att(2, 4)
-    send_heads(1)
+    send_heads(2, 4)
     att(4, 6)
-    depart("2")
+    depart("c")
+    depart("d")
     relay("0", 0)
     relay("0", 1)
     att(6, 7)
+    spread_shares()
     arrive("1")
     gather_x("1")
     gather_y("1")
@@ -529,101 +552,107 @@
     keep.wait()
     core_near("0")
     core_far("0")
+    swap_shares()
     relay("1", 0)
     relay("1", 1)
     depart("a")
     depart("b")
     core_near("1")
-    arrive("2")
-    gather_x("2")
-    gather_y("2")
-    send_heads(2)
+    arrive("c")
+    gather_x("c")
+    gather_y("c")
+    arrive("d")
+    gather_x("d")
+    gather_y("d")
+    send_heads(4, 6)
+    take_shares()
     up("0", 0)
     up("0", 1)
-    relay("2", 0)
-    relay("2", 1)
-    core_near("2")
+    relay("c", 0)
+    core_near("c")
+    relay("d", 0)
+    core_near("d")
     arrive("a")
     gather_x("a")
     gather_y("a")
     arrive("b")
     gather_x("b")
     gather_y("b")
-    send_heads(3)
-    send_heads(0)
+    send_heads(6, 8)
+    send_heads(0, 2)
     core_far("1")
     down("0")
-    up("1", 0)
+    experts("1")
     relay("a", 0)
     core_near("a")
-    up("1", 1)
+    core_far("c")
     relay("b", 0)
     core_near("b")
-    down("1")
-    core_far("2")
+    core_far("d")
     scatter("1")
-    up("2", 0)
-    up("2", 1)
+    experts("c")
     core_far("a")
-    down("2")
+    up("d", 0)
+    up("d", 1)
     core_far("b")
+    scatter("c")
+    down("d")
     scatter_relay("1")
-    scatter("2")
     relay_heads()
-    experts("a")
+    up("a", 0)
+    up("a", 1)
+    scatter("d")
+    down("a")
+    scatter_relay("c")
     experts("b")
     scatter("a")
-    scatter_relay("2")
+    await_heads()
     home("1")
     scatter("b")
+    scatter_relay("d")
+    project(0)
+    home("c")
+    project(1)
     scatter_relay("a")
     scatter_far("0")
-    await_heads()
-    home("2")
-    project(0)
+    project(2)
+    home("d")
+    project(3)
     scatter_relay("b")
     scatter_near("0")
     home("a")
-    project(1)
     scatter_relay("0")
-    project(2)
     home("b")
-    project(3)
     home("0")
-    settle("1")
-    settle("2")
-    settle("a")
-    settle("b")
-    with NS("finish"):
-        moved[...] = lax.dot_general(
-            take, back[...], (((0,), (0,)), ((), ())), preferred_element_type=jnp.float32
-        ).astype(jnp.bfloat16)
+    settle()
     with NS("wsend"):
         for copy in in_flight.values():
             copy.wait_send()
 
 
-def store_kernel(mixed, moved, mixer_hbm, out_hbm, sem):
-    copies = [
-        pltpu.make_async_copy(source, target, sem.at[i])
-        for i, (source, target) in enumerate(((mixed, mixer_hbm), (moved, out_hbm)))
-    ]
-    for copy in copies:
-        copy.start()
-    for copy in copies:
-        copy.wait()
-
-
-def store(mixed, moved):
+def store_kernel(mixed, back, take, mixer_hbm, out_hbm, moved, sem):
+    mixer_copy = pltpu.make_async_copy(mixed, mixer_hbm, sem.at[0])
+    mixer_copy.start()
+    moved[...] = lax.dot_general(
+        take[...], back[...], (((0,), (0,)), ((), ())), preferred_element_type=jnp.float32
+    ).astype(jnp.bfloat16)
+    out_copy = pltpu.make_async_copy(moved, out_hbm, sem.at[1])
+    out_copy.start()
+    mixer_copy.wait()
+    out_copy.wait()
+
+
+def store(mixed, back, take):
     anywhere = pl.BlockSpec(memory_space=pl.ANY)
+    vmem = pl.BlockSpec(memory_space=pltpu.VMEM)
     return pl.pallas_call(
         store_kernel,
-        out_shape=tuple(jax.ShapeDtypeStruct(v.shape, v.dtype) for v in (mixed, moved)),
-        in_specs=[anywhere] * 2,
+        out_shape=tuple(jax.ShapeDtypeStruct(v.shape, v.dtype) for v in (mixed, back)),
+        in_specs=[anywhere, vmem, vmem],
         out_specs=(anywhere, anywhere),
-        scratch_shapes=[pltpu.SemaphoreType.DMA((2,))],
-        compiler_params=pltpu.CompilerParams(vmem_limit_bytes=2**20),
-    )(*(pltpu.with_memory_space_constraint(v, pltpu.VMEM) for v in (mixed, moved)))
+        scratch_shapes=[pltpu.VMEM(back.shape, back.dtype), pltpu.SemaphoreType.DMA((2,))],
+        compiler_params=pltpu.CompilerParams(vmem_limit_bytes=8 * 2**20),
+    )(*(pltpu.with_memory_space_constraint(v, pltpu.VMEM) for v in (mixed, back, take)))
 
 
 def fused(
@@ -644,20 +673,20 @@
     groups = router_group.shape[1]
     block = tokens_b.shape[0] // 4
     experts, depth, hidden = expert_gate.shape
-    width = depth + LANES
     row_count, head_width = q_heads.shape
     down = expert_down.reshape(experts * hidden, depth)
     chunk = block // groups
     bf16 = jnp.bfloat16
     anywhere = pl.BlockSpec(memory_space=pl.ANY)
-    mixed, moved = pl.pallas_call(
+    mixed, back, take = pl.pallas_call(
         functools.partial(fused_kernel, groups),
         out_shape=(
             pltpu.VMEM((row_count, proj.shape[1]), bf16),
             pltpu.VMEM((block, depth), bf16),
+            pltpu.VMEM((block, block), bf16),
         ),
         in_specs=[anywhere] * 13,
-        out_specs=(pl.BlockSpec(memory_space=pltpu.VMEM),) * 2,
+        out_specs=(pl.BlockSpec(memory_space=pltpu.VMEM),) * 3,
         scratch_shapes=[
             pltpu.SMEM(sinks.shape, jnp.float32),
             pltpu.VMEM(q_heads.shape, bf16),
@@ -668,9 +697,10 @@
             pltpu.VMEM((HD, row_count + WINDOW), bf16),
             pltpu.VMEM((HD, row_count + WINDOW), bf16),
             pltpu.VMEM((block, depth), bf16),
-            pltpu.VMEM((block, width), bf16),
+            pltpu.VMEM((block, depth), bf16),
+            pltpu.VMEM((groups, 8, 2 * (router_expert.shape[1] // groups), block), bf16),
             pltpu.VMEM((4, row_count, head_width), bf16),
-            pltpu.VMEM((groups, 8, chunk, width), bf16),
+            pltpu.VMEM((groups, 8, chunk, depth), bf16),
             pltpu.VMEM((groups, 8, chunk, depth), bf16),
             pltpu.VMEM(expert_gate.shape, bf16),
             pltpu.VMEM(expert_up.shape, bf16),
@@ -682,7 +712,6 @@
             pltpu.VMEM((groups, chunk, depth // 2), bf16),
             pltpu.VMEM((groups, 2, chunk, depth), bf16),
             pltpu.VMEM((groups, chunk, depth), bf16),
-            pltpu.VMEM((block, depth), bf16),
             pltpu.SemaphoreType.DMA((13,)),
             pltpu.SemaphoreType.DMA((1,)),
             pltpu.SemaphoreType.DMA((SENDERS,)),
@@ -714,7 +743,7 @@
             )
         )
     )
-    return store(mixed, moved)
+    return store(mixed, back, take)
 
 
 def per_device(

time: 56.1 us -> 53.8 us (0.959)
  Pallas kernels: 55.3 us -> 53 us
    pallas_call x1, Pallas kernels: 54.1 us -> 51.9 us  [fused(): pl.pallas_call(functools.partial(fused_kernel, groups), out_shape=(pltpu....]
where the time goes in v3:
time: 53.8 us; the launch traced here: 53.7 us
  Pallas kernels  53 us (99%)
  between operations  0.64 us (1%)
    pallas_call x1, Pallas kernels, fused(): pl.pallas_call(functools.partial(fused_kernel, groups), out_shape=(pltpu....  51.9 us
    pallas_call x1, Pallas kernels, store(): pl.pallas_call(store_kernel, out_shape=tuple((jax.ShapeDtypeStruct(v.shap...  1.16 us

profile of v3, /device:TPU:0, one launch (start us, length us, event | category | flops | bytes accessed | tf_op | source)
XLA Modules:
  0.0 53.7 jit_solution(5333609394152738128)
XLA Ops:
  0.6 51.9 %shard_map.140 = (bf16[1024,512]{1,0:T(8,128)(2,1)S(1)}, bf16[128,2048]{1,0:T(8,128)(2,1)S(1)}, bf16[128,128]{1,0:T(8,128)(2,1)S(1)}) custom-call(f32[4]{0:T(128)} %sink_hbm.1, bf16[1024,256]{1,0:T(8,128)(2,1)} %q_hbm.1, bf16[64,1024]{1,0:T(8,128)(2,1)} %bitcast.8, bf16[64,1024]{1,0:T(8,128)(2,1)} %bitcast.9, f32[1,2048]{1,0:T(1,128)} %bitcast.12, ...), custom_call_target="tpu_custom_call" | custom-call | flops 20000000000 | bytes 20000000 | tf_op jit(solution)/shard_map/pallas_call | solution.py:681
  52.5 1.2 %shard_map.141 = (bf16[1024,512]{1,0:T(8,128)(2,1)}, bf16[128,2048]{1,0:T(8,128)(2,1)}) custom-call(bf16[1024,512]{1,0:T(8,128)(2,1)S(1)} %get-tuple-element.5.mixed, bf16[128,2048]{1,0:T(8,128)(2,1)S(1)} %get-tuple-element.6.back, bf16[128,128]{1,0:T(8,128)(2,1)S(1)} %get-tuple-element.7.take), custom_call_target="tpu_custom_call" | custom-call | tf_op jit(solution)/shard_map/pallas_call | solution.py:648

commit v4 on v3

--- a/solution.py
+++ b/solution.py
@@ -186,7 +186,7 @@
         for i, (source, held) in enumerate(pairs)
     ]
     early, middle, late = loads[:5], loads[5:9], loads[9:]
-    for load in early + middle:
+    for load in early:
         load.start()
     early[4].wait()
     routes = route_ref[...]
@@ -207,7 +207,7 @@
     with NS("wearly"):
         for load in early[:4]:
             load.wait()
-    for load in late:
+    for load in middle + late:
         load.start()
     values = tokens[...].astype(jnp.float32)
     scale = lax.rsqrt(jnp.mean(values * values, axis=1, keepdims=True) + 1e-06)
@@ -271,11 +271,14 @@
         receive(f"z{u}", rows.at[s, own, span_of(u)])
 
     def gather_x(u):
+        for i in range(units[u][2] // piece_rows):
+            gather_piece(u, i)
+
+    def gather_piece(u, i):
         s, begin, count = units[u]
-        for i in range(count // piece_rows):
-            at = begin + i * piece_rows
-            target = rows.at[s, own, pl.ds(at, piece_rows)]
-            send(f"x{u}{i}", own_rows(s, at, piece_rows), target, x_dev)
+        at = begin + i * piece_rows
+        target = rows.at[s, own, pl.ds(at, piece_rows)]
+        send(f"x{u}{i}", own_rows(s, at, piece_rows), target, x_dev)
 
     def gather_y(u):
         s, begin, count = units[u]
@@ -463,7 +466,7 @@
                 jnp.bfloat16
             )
 
-    gather_x(FIRST)
+    gather_piece(FIRST, 0)
     gather_y(FIRST)
     depart("1")
     group_logits = lax.dot_general(
@@ -497,6 +500,8 @@
     for step in range(1, groups):
         there = (plane(step) * 2 + member, tp)
         send("share_z", share_ref.at[0, own], share_ref.at[step, own], there)
+
+    gather_piece(FIRST, 1)
 
     def spread_shares():
         receive("share_z", share_ref.at[pl.ds(1, groups - 1), own])
@@ -551,6 +556,7 @@
     take_weights()
     keep.wait()
     core_near("0")
+    send_heads(4, 6)
     core_far("0")
     swap_shares()
     relay("1", 0)
@@ -564,7 +570,6 @@
     arrive("d")
     gather_x("d")
     gather_y("d")
-    send_heads(4, 6)
     take_shares()
     up("0", 0)
     up("0", 1)
@@ -582,42 +587,53 @@
     send_heads(0, 2)
     core_far("1")
     down("0")
-    experts("1")
+    up("1", 0)
+    up("1", 1)
+    down("1")
     relay("a", 0)
     core_near("a")
     core_far("c")
     relay("b", 0)
     core_near("b")
     core_far("d")
-    scatter("1")
-    experts("c")
+    scatter_far("1")
+    scatter_near("1")
+    up("c", 0)
+    up("c", 1)
+    down("c")
     core_far("a")
     up("d", 0)
     up("d", 1)
     core_far("b")
-    scatter("c")
+    scatter_far("c")
     down("d")
     scatter_relay("1")
+    scatter_near("c")
     relay_heads()
     up("a", 0)
     up("a", 1)
-    scatter("d")
+    scatter_far("d")
+    scatter_near("d")
     down("a")
     scatter_relay("c")
-    experts("b")
-    scatter("a")
+    up("b", 0)
+    up("b", 1)
+    scatter_far("a")
+    scatter_near("a")
+    down("b")
     await_heads()
     home("1")
-    scatter("b")
+    scatter_far("b")
+    scatter_near("b")
     scatter_relay("d")
     project(0)
     home("c")
+    scatter_far("0")
     project(1)
+    project(3)
     scatter_relay("a")
-    scatter_far("0")
     project(2)
     home("d")
-    project(3)
     scatter_relay("b")
     scatter_near("0")
     home("a")

time: 53.8 us -> 53.3 us (level)
  no operation moved by 1% of the time
where the time goes in v4:
time: 53.3 us; the launch traced here: 53.1 us
  Pallas kernels  52.5 us (98%)
  between operations  0.64 us (1%)
    pallas_call x1, Pallas kernels, fused(): pl.pallas_call(functools.partial(fused_kernel, groups), out_shape=(pltpu....  51.3 us
    pallas_call x1, Pallas kernels, store(): pl.pallas_call(store_kernel, out_shape=tuple((jax.ShapeDtypeStruct(v.shap...  1.16 us

profile of v4, /device:TPU:0, one launch (start us, length us, event | category | flops | bytes accessed | tf_op | source)
XLA Modules:
  0.0 53.1 jit_solution(8767194626042613424)
XLA Ops:
  0.6 51.3 %shard_map.140 = (bf16[1024,512]{1,0:T(8,128)(2,1)S(1)}, bf16[128,2048]{1,0:T(8,128)(2,1)S(1)}, bf16[128,128]{1,0:T(8,128)(2,1)S(1)}) custom-call(f32[4]{0:T(128)} %sink_hbm.1, bf16[1024,256]{1,0:T(8,128)(2,1)} %q_hbm.1, bf16[64,1024]{1,0:T(8,128)(2,1)} %bitcast.8, bf16[64,1024]{1,0:T(8,128)(2,1)} %bitcast.9, f32[1,2048]{1,0:T(1,128)} %bitcast.12, ...), custom_call_target="tpu_custom_call" | custom-call | flops 20000000000 | bytes 20000000 | tf_op jit(solution)/shard_map/pallas_call | solution.py:697
  52.0 1.2 %shard_map.141 = (bf16[1024,512]{1,0:T(8,128)(2,1)}, bf16[128,2048]{1,0:T(8,128)(2,1)}) custom-call(bf16[1024,512]{1,0:T(8,128)(2,1)S(1)} %get-tuple-element.5.mixed, bf16[128,2048]{1,0:T(8,128)(2,1)S(1)} %get-tuple-element.6.back, bf16[128,128]{1,0:T(8,128)(2,1)S(1)} %get-tuple-element.7.take), custom_call_target="tpu_custom_call" | custom-call | tf_op jit(solution)/shard_map/pallas_call | solution.py:664

commit v5 on v4

--- a/solution.py
+++ b/solution.py
@@ -72,8 +72,8 @@
     pl.delay(1)
 
 FIRST = "0"
-SENDERS = 24
-RECEIVERS = 58
+SENDERS = 20
+RECEIVERS = 56
 
 
 def UNITS(chunk):
@@ -448,15 +448,14 @@
         send("heads_x", heads.at[tp, span], heads.at[tp, span], x_dev)
 
     def share_heads():
-        send("heads_c", heads.at[tp], heads.at[tp], c_dev)
+        send("heads", heads.at[tp], heads.at[tp], c_dev)
 
     def relay_heads():
         receive("heads_x", heads.at[tp_x])
-        send("heads_cx", heads.at[tp_x], heads.at[tp_x], c_dev)
+        send("heads", heads.at[tp_x], heads.at[tp_x], c_dev)
 
     def await_heads():
-        receive("heads_c", heads.at[tp_c])
-        receive("heads_cx", heads.at[tp_c])
+        receive("heads", heads.at[pl.ds(0, 2)])
 
     def project(i):
         span = pl.ds(i * piece, piece)
@@ -521,15 +520,14 @@
         for load in middle:
             load.wait()
     for name, ext in (("k", k_ext), ("v", v_ext)):
-        send("halo" + name, ext.at[:, pl.ds(row_count, WINDOW)], ext.at[:, pl.ds(0, WINDOW)], next_dev)
+        send("halo", ext.at[:, pl.ds(row_count, WINDOW)], ext.at[:, pl.ds(0, WINDOW)], next_dev)
     keep = pltpu.make_async_copy(
         xs_ref.at[pl.ds(my_start, chunk)], rows.at[0, own], out_sem.at[0]
     )
     keep.start()
 
     def take_halo():
-        for name, ext in (("k", k_ext), ("v", v_ext)):
-            receive("halo" + name, ext.at[:, pl.ds(0, WINDOW)])
+        receive("halo", k_ext.at[:, pl.ds(0, 2 * WINDOW)])
 
     def take_weights():
         with NS("loads"):

time: 53.3 us -> 53.3 us (level)
  no operation moved by 1% of the time
where the time goes in v5:
time: 53.3 us; the launch traced here: 53.1 us
  Pallas kernels  52.4 us (98%)
  between operations  0.64 us (1%)
    pallas_call x1, Pallas kernels, fused(): pl.pallas_call(functools.partial(fused_kernel, groups), out_shape=(pltpu....  51.3 us
    pallas_call x1, Pallas kernels, store(): pl.pallas_call(store_kernel, out_shape=tuple((jax.ShapeDtypeStruct(v.shap...  1.16 us

profile of v5, /device:TPU:0, one launch (start us, length us, event | category | flops | bytes accessed | tf_op | source)
XLA Modules:
  0.0 53.1 jit_solution(6442246388006533635)
XLA Ops:
  0.6 51.3 %shard_map.140 = (bf16[1024,512]{1,0:T(8,128)(2,1)S(1)}, bf16[128,2048]{1,0:T(8,128)(2,1)S(1)}, bf16[128,128]{1,0:T(8,128)(2,1)S(1)}) custom-call(f32[4]{0:T(128)} %sink_hbm.1, bf16[1024,256]{1,0:T(8,128)(2,1)} %q_hbm.1, bf16[64,1024]{1,0:T(8,128)(2,1)} %bitcast.8, bf16[64,1024]{1,0:T(8,128)(2,1)} %bitcast.9, f32[1,2048]{1,0:T(1,128)} %bitcast.12, ...), custom_call_target="tpu_custom_call" | custom-call | flops 20000000000 | bytes 20000000 | tf_op jit(solution)/shard_map/pallas_call | solution.py:695
  51.9 1.2 %shard_map.141 = (bf16[1024,512]{1,0:T(8,128)(2,1)}, bf16[128,2048]{1,0:T(8,128)(2,1)}) custom-call(bf16[1024,512]{1,0:T(8,128)(2,1)S(1)} %get-tuple-element.5.mixed, bf16[128,2048]{1,0:T(8,128)(2,1)S(1)} %get-tuple-element.6.back, bf16[128,128]{1,0:T(8,128)(2,1)S(1)} %get-tuple-element.7.take), custom_call_target="tpu_custom_call" | custom-call | tf_op jit(solution)/shard_map/pallas_call | solution.py:662
